TPU v7x, 32 devices: a whole 2x2x4 slice. The times are simulated.
32 devices in a mesh: ep: 16 (over z, y, x), tp: 2 (over core).
Axes of the slice: x: 2, y: 2, z: 4, core: 2. Of those that a mesh axis runs over, the one named last changes fastest.
Arguments:
- tokens: bfloat16 [4096, 2048], P(('ep', 'tp')), may hold values from -6 to 6
- norm_gain: float32 [2048], replicated, may hold values from 0.25 to 4
- routes: int32 [4096, 2], P(('ep', 'tp')), may hold values from 0 to 15, all different within a row; in each aligned block of 128 rows (0 to 127, 128 to 255, ...) at most 22 rows name the same one
- route_weights: float32 [4096, 2], P(('ep', 'tp')), may hold values from 0.1 to 1
- w_gate: bfloat16 [16, 2048, 1024], P('ep', None, 'tp'), may hold values from -0.125 to 0.125
- w_up: bfloat16 [16, 2048, 1024], P('ep', None, 'tp'), may hold values from -0.125 to 0.125
- w_down: bfloat16 [16, 1024, 2048], P('ep', 'tp'), may hold values from -0.1875 to 0.1875
- dense_in: bfloat16 [2048, 256], P('ep'), may hold values from -0.125 to 0.125
- dense_out: bfloat16 [2048, 256], P('ep'), may hold values from -0.375 to 0.375
- dense_gate: float32 [2048], replicated, may hold values from -6 to 6
Outputs:
- mixed: bfloat16 [4096, 2048], P(('ep', 'tp'))
Inputs may be any that keep to these rules, and one draw needn't show every extreme that they name: `routes`: each row names 2 different experts. Among the 128 rows of one device no expert is named more than 22 times; every draw has a device and an expert with exactly 22.
All inputs are finite; a program needn't handle non-finite values.
Results may differ from a plain program's by a relative error of at most 0.0074.
Values may be sent and summed in bfloat16 or wider, within the bound.
A program may use at most 128 MiB of HBM per device.

v0:
```python
import functools
import math

import jax
import jax.numpy as jnp
from jax import lax
from jax.experimental import pallas as pl
from jax.experimental.pallas import tpu as pltpu
from jax.sharding import PartitionSpec as P

CLAMP_LIMIT = 7.0
SLOPE_ALPHA = 1.702
NORM_EPS = 1e-06
MESH = pl.DeviceIdType.MESH
F32 = jnp.float32
BF16 = jnp.bfloat16


def clamped_unit(gate_pre, up_pre):
    gate_clip = jnp.minimum(gate_pre, CLAMP_LIMIT)
    up_clip = jnp.clip(up_pre, -CLAMP_LIMIT, CLAMP_LIMIT)
    return ((up_clip + 1.0) * gate_clip * jax.nn.sigmoid(SLOPE_ALPHA * gate_clip)).astype(BF16)


def layer_kernel(
    sizes,
    routes_t_ref,
    routes_ref,
    weights_ref,
    tokens_ref,
    gain_ref,
    dgate_ref,
    din_ref,
    dout_ref,
    wg_ref,
    wu_ref,
    wd_ref,
    out_ref,
    normed,
    keys,
    stacked,
    places,
    xs,
    totals,
    unpack_ref,
    pack_ref,
    buf,
    recv,
    outb,
    ret,
    wgs,
    wus,
    wds,
    hid,
    dn,
    acc,
    send1,
    recv1,
    send2,
    recv2,
    w_local,
    w_send,
    w_recv,
    ds1,
    dr1,
    ds2,
    dr2,
    ds3,
    dr3,
):
    n, n1, n2, cap, blocks = sizes
    rows, width = tokens_ref.shape
    half = wg_ref.shape[1]
    tall, tile = blocks * cap, width // blocks
    group_rows, packed_rows = n2 * cap, n2 * blocks * cap
    me = lax.axis_index("ep")
    core = lax.axis_index("tp")
    plane, spot = me // n2, me % n2
    peer = 1 - core

    barrier = pltpu.get_barrier_semaphore()

    def greet(i, carry):
        pl.semaphore_signal(
            barrier, inc=1, device_id={"ep": (me + i) % n}, device_id_type=MESH
        )
        return carry

    lax.fori_loop(1, n, greet, 0)
    pl.semaphore_signal(barrier, inc=1, device_id={"tp": peer}, device_id_type=MESH)

    weight_pairs = ((wg_ref, wgs), (wu_ref, wus), (wd_ref, wds))
    for i, (src, dst) in enumerate(weight_pairs):
        pltpu.make_async_copy(src, dst.at[0], w_local.at[i]).start()

    @pl.when(core == 0)
    def _():
        dn[0, plane, spot] = din_ref[...]

    @pl.when(core == 1)
    def _():
        dn[1, plane, spot] = dout_ref[...]

    widened = tokens_ref[...].astype(F32)
    inv_scale = lax.rsqrt(jnp.mean(widened * widened, axis=1, keepdims=True) + NORM_EPS)
    normed[...] = (widened * inv_scale * gain_ref[...]).astype(BF16)
    for j in range(blocks):
        stacked[j * rows : (j + 1) * rows, :] = normed[:, j * tile : (j + 1) * tile]

    expert_ids = lax.broadcasted_iota(jnp.int32, (n, rows), 0)
    chosen = (routes_t_ref[0:1, :] == expert_ids) | (routes_t_ref[1:2, :] == expert_ids)
    earlier = (
        lax.broadcasted_iota(jnp.int32, (rows, rows), 0)
        < lax.broadcasted_iota(jnp.int32, (rows, rows), 1)
    )
    counted = jnp.dot(
        jnp.where(chosen, 1.0, 0.0).astype(BF16),
        jnp.where(earlier, 1.0, 0.0).astype(BF16),
        preferred_element_type=F32,
    )
    for j in range(blocks):
        found = jnp.where(chosen, counted.astype(jnp.int32) + j * cap, -1)
        for z in range(n1):
            keys[z, :, j * rows : (j + 1) * rows] = found[z * n2 : (z + 1) * n2]
    experts_across = lax.broadcasted_iota(jnp.int32, (rows, n), 1)
    takes = [routes_ref[:, k : k + 1] == experts_across for k in range(2)]
    before = (
        lax.broadcasted_iota(jnp.int32, (rows, rows), 0)
        > lax.broadcasted_iota(jnp.int32, (rows, rows), 1)
    )
    counts = jnp.dot(
        jnp.where(before, 1.0, 0.0).astype(BF16),
        jnp.where(takes[0] | takes[1], 1.0, 0.0).astype(BF16),
        preferred_element_type=F32,
    )
    for k in range(2):
        slot = jnp.sum(jnp.where(takes[k], counts, 0.0), axis=1, keepdims=True)
        places[:, k : k + 1] = routes_ref[:, k : k + 1] * tall + slot.astype(jnp.int32)

    pl.semaphore_wait(barrier, n)

    def weight_copy(i):
        src, dst = weight_pairs[i]
        return pltpu.make_async_remote_copy(
            src_ref=src,
            dst_ref=dst.at[1],
            send_sem=w_send.at[i],
            recv_sem=w_recv.at[i],
            device_id={"tp": peer},
            device_id_type=MESH,
        )

    def dense_copy1(bit, block):
        other = plane + bit - 2 * bit * ((plane // bit) % 2)
        return pltpu.make_async_remote_copy(
            src_ref=dn.at[core, block, spot],
            dst_ref=dn.at[core, block, spot],
            send_sem=ds1.at[block],
            recv_sem=dr1.at[block],
            device_id={"ep": other * n2 + spot},
            device_id_type=MESH,
        )

    bits = [1 << b for b in reversed(range(n1.bit_length() - 1))]

    def dense_held(bit, where):
        return [where % (2 * bit) + m * 2 * bit for m in range(n1 // (2 * bit))]

    def dense_start(bit):
        for block in dense_held(bit, plane):
            dense_copy1(bit, block).start()

    def dense_finish(bit):
        for block in dense_held(bit, plane + bit - 2 * bit * ((plane // bit) % 2)):
            dense_copy1(bit, block).wait_recv()
        for block in dense_held(bit, plane):
            dense_copy1(bit, block).wait_send()

    def dense_copy2(other, slot):
        return pltpu.make_async_remote_copy(
            src_ref=dn.at[core, :, slot],
            dst_ref=dn.at[core, :, slot],
            send_sem=ds2.at[other],
            recv_sem=dr2.at[slot],
            device_id={"ep": plane * n2 + other},
            device_id_type=MESH,
        )

    def dense_copy3(which):
        return pltpu.make_async_remote_copy(
            src_ref=dn.at[which],
            dst_ref=dn.at[which],
            send_sem=ds3,
            recv_sem=dr3,
            device_id={"tp": peer},
            device_id_type=MESH,
        )

    def each(count, act):
        def step(i, carry):
            act(i)
            return carry

        lax.fori_loop(0, count, step, 0)

    dense_start(bits[0])
    for i in range(3):
        weight_copy(i).start()

    def dispatch(dst, slot):
        return pltpu.make_async_remote_copy(
            src_ref=buf.at[dst],
            dst_ref=recv.at[slot],
            send_sem=send1.at[dst],
            recv_sem=recv1.at[slot],
            device_id={"ep": dst},
            device_id_type=MESH,
        )

    def give_back(dst, slot):
        return pltpu.make_async_remote_copy(
            src_ref=outb.at[dst],
            dst_ref=ret.at[slot],
            send_sem=send2.at[dst],
            recv_sem=recv2.at[slot],
            device_id={"ep": dst},
            device_id_type=MESH,
        )

    def partner_plane(x):
        return sum(((plane // b) % 2 + (x // b) % 2) % 2 * b for b in bits)

    def turn(i):
        return partner_plane(i % 2 * (n1 // 2) + i // 2)

    def send_group(i):
        group = partner_plane((i + n1 // 2) % n1)
        first = group * n2
        wanted = keys[group]
        picks = wanted[:, None, :] == lax.broadcasted_iota(
            jnp.int32, (n2, tall, blocks * rows), 1
        )
        picks = jnp.where(picks, 1.0, 0.0).reshape(packed_rows, blocks * rows).astype(BF16)
        found = jnp.dot(picks, stacked[...], preferred_element_type=F32)
        buf[pl.ds(first, n2)] = found.reshape(n2, tall, tile).astype(BF16)

        def start(j):
            dst = first + (spot + 1 + j) % n2

            @pl.when(dst != me)
            def _():
                dispatch(dst, me).start()

            @pl.when(dst == me)
            def _():
                recv[me] = buf[me]

        each(n2, start)

    each(n1, send_group)


    for i, (src, dst) in enumerate(weight_pairs):
        pltpu.make_async_copy(src, dst.at[0], w_local.at[i]).wait()
    for i in range(3):
        weight_copy(i).wait()

    piece = min(256, half)
    upright = lax.broadcasted_iota(jnp.int32, (packed_rows, packed_rows), 0)
    across = lax.broadcasted_iota(jnp.int32, (packed_rows, packed_rows), 1)

    def packed_place(r):
        return (r // cap) % n2 * tall + r // group_rows * cap + r % cap

    unpack = jnp.where(packed_place(upright) == across, 1.0, 0.0).astype(BF16)
    pack = jnp.where(packed_place(across) == upright, 1.0, 0.0).astype(BF16)
    unpack_ref[...] = unpack
    pack_ref[...] = pack

    def run_group(i):
        group = turn(i)
        first = group * n2

        def arrive(j):
            src = first + j

            @pl.when(src != me)
            def _():
                dispatch(src, src).wait_recv()

        each(n2, arrive)
        came = recv[pl.ds(first, n2)].astype(F32).reshape(packed_rows, tile).astype(BF16)
        apart = jnp.dot(unpack_ref[...], came, preferred_element_type=F32)
        for j in range(blocks):
            xs[:, j * tile : (j + 1) * tile] = apart[
                j * group_rows : (j + 1) * group_rows
            ].astype(BF16)
        x = xs[...]
        for part in range(2):
            for low in range(0, half, piece):
                gate_pre = jnp.dot(
                    x, wgs[part, :, low : low + piece], preferred_element_type=F32
                )
                up_pre = jnp.dot(x, wus[part, :, low : low + piece], preferred_element_type=F32)
                hid[part, :, low : low + piece] = clamped_unit(gate_pre, up_pre)
        for j in range(blocks):
            total = jnp.zeros((group_rows, tile), F32)
            for part in range(2):
                partial = jnp.dot(
                    hid[part],
                    wds[part, :, j * tile : (j + 1) * tile],
                    preferred_element_type=F32,
                )
                total = total + partial.astype(BF16).astype(F32)
            totals[j * group_rows : (j + 1) * group_rows, :] = total
        joined = jnp.dot(pack_ref[...], totals[...].astype(BF16), preferred_element_type=F32)
        outb[pl.ds(first, n2)] = joined.reshape(n2, tall, tile).astype(BF16)

        def start(j):
            dst = first + (spot + 1 + j) % n2

            @pl.when(dst != me)
            def _():
                give_back(dst, me).start()

            @pl.when(dst == me)
            def _():
                ret[me] = outb[me]

        each(n2, start)

    def run_turn(i):
        run_group(i)
        for b, bit in enumerate(bits):

            @pl.when(i == b)
            def _():
                dense_finish(bit)
                if b + 1 < len(bits):
                    dense_start(bits[b + 1])
                else:
                    each(n2 - 1, lambda j: dense_copy2((spot + 1 + j) % n2, spot).start())

    each(n1, run_turn)
    each(n2 - 1, lambda i: dense_copy2((spot + 1 + i) % n2, (spot + 1 + i) % n2).wait_recv())
    dense_copy3(core).start()
    dense_copy3(core).wait_send()
    dense_copy3(peer).wait_recv()
    depth = din_ref.shape[1]
    dense_pre = jnp.dot(
        normed[...], dn[0].reshape(width, depth), preferred_element_type=F32
    )
    dense_hidden = jax.nn.silu(dense_pre).astype(BF16)
    step = width // n1
    for z in range(n1):
        branch = lax.dot_general(
            dense_hidden,
            dn[1, z].reshape(step, depth),
            (((1,), (1,)), ((), ())),
            preferred_element_type=F32,
        )
        acc[:, z * step : (z + 1) * step] = (
            jax.nn.sigmoid(dgate_ref[:, z * step : (z + 1) * step]) * branch
        )

    def combine_group(i):
        group = turn(i)
        first = group * n2

        def arrive(j):
            src = first + j

            @pl.when(src != me)
            def _():
                give_back(src, src).wait_recv()

        each(n2, arrive)
        back = ret[pl.ds(first, n2)].astype(F32).reshape(packed_rows, tile).astype(BF16)
        lanes = lax.broadcasted_iota(jnp.int32, (rows, packed_rows), 1) + first * tall
        wanted = jnp.concatenate(
            [
                jnp.where(places[:, k : k + 1] + j * cap == lanes, 1.0, 0.0).astype(BF16)
                for k in range(2)
                for j in range(blocks)
            ],
            axis=0,
        )
        picked = jnp.dot(wanted, back, preferred_element_type=F32)
        for j in range(blocks):
            total = acc[:, j * tile : (j + 1) * tile]
            for k in range(2):
                at = (k * blocks + j) * rows
                total = total + picked[at : at + rows] * weights_ref[:, k : k + 1]
            acc[:, j * tile : (j + 1) * tile] = total

    each(n1, combine_group)
    out_ref[...] = acc[...].astype(BF16)

    def drain(i):
        other = (me + 1 + i) % n
        dispatch(other, me).wait_send()
        give_back(other, me).wait_send()

    each(n - 1, drain)
    each(n2 - 1, lambda i: dense_copy2((spot + 1 + i) % n2, spot).wait_send())


def shards(
    tokens, norm_gain, routes, route_weights, w_gate, w_up, w_down, dense_in, dense_out, dense_gate
):
    rows, width = tokens.shape
    top_count = routes.shape[1]
    n = lax.axis_size("ep")
    capacity = (4 * rows * top_count + 3 * n - 1) // (3 * n)
    cap = capacity
    blocks = 8 // math.gcd(cap, 8)
    tall, tile = blocks * cap, width // blocks
    n2 = 1
    while n2 * n2 < n:
        n2 *= 2
    n1 = n // n2
    half = w_gate.shape[2]
    depth = dense_in.shape[1]
    vmem = pl.BlockSpec(memory_space=pltpu.VMEM)
    anywhere = pl.BlockSpec(memory_space=pl.ANY)
    dma = pltpu.SemaphoreType.DMA
    slab = pltpu.VMEM((n, tall, tile), BF16)
    return pl.pallas_call(
        functools.partial(layer_kernel, (n, n1, n2, cap, blocks)),
        out_shape=jax.ShapeDtypeStruct((rows, width), BF16),
        in_specs=[vmem] * 8 + [anywhere] * 3,
        out_specs=vmem,
        scratch_shapes=[
            pltpu.VMEM((rows, width), BF16),
            pltpu.VMEM((n1, n2, blocks * rows), jnp.int32),
            pltpu.VMEM((blocks * rows, tile), BF16),
            pltpu.VMEM((rows, 2), jnp.int32),
            pltpu.VMEM((n2 * cap, width), BF16),
            pltpu.VMEM((n2 * tall, tile), F32),
            pltpu.VMEM((n2 * tall, n2 * tall), BF16),
            pltpu.VMEM((n2 * tall, n2 * tall), BF16),
            slab,
            slab,
            slab,
            slab,
            pltpu.VMEM((2, width, half), BF16),
            pltpu.VMEM((2, width, half), BF16),
            pltpu.VMEM((2, half, width), BF16),
            pltpu.VMEM((2, n2 * cap, half), BF16),
            pltpu.VMEM((2, n1, n2, width // n, depth), BF16),
            pltpu.VMEM((rows, width), F32),
            dma((n,)),
            dma((n,)),
            dma((n,)),
            dma((n,)),
            dma((3,)),
            dma((3,)),
            dma((3,)),
            dma((n1,)),
            dma((n1,)),
            dma((n2,)),
            dma((n2,)),
            dma,
            dma,
        ],
        compiler_params=pltpu.CompilerParams(
            collective_id=0, has_side_effects=True, vmem_limit_bytes=60 * 1024 * 1024
        ),
    )(
        routes.T,
        routes,
        route_weights,
        tokens,
        norm_gain.reshape(1, width),
        dense_gate.reshape(1, width),
        dense_in,
        dense_out,
        w_gate[0],
        w_up[0],
        w_down[0],
    )


def solution(mesh):
    placed = (
        P(("ep", "tp"), None),
        P(),
        P(("ep", "tp"), None),
        P(("ep", "tp"), None),
        P("ep", None, "tp"),
        P("ep", None, "tp"),
        P("ep", "tp", None),
        P("ep", None),
        P("ep", None),
        P(),
    )
    return jax.shard_map(
        shards, mesh=mesh, in_specs=placed, out_specs=P(("ep", "tp"), None), check_vma=False
    )
```

profile of v0, /device:TPU:9, one launch (start us, length us, event | category | flops | bytes accessed | tf_op | source)
XLA Modules:
  0.0 79.3 jit_solution(5958335598028530581)
XLA Ops:
  0.0 1.4 %copy.12.weights_ref = f32[128,2]{1,0:T(8,128)} copy(f32[128,2]{0,1:T(2,128)} %param.13) | data formatting | bytes 2048 | tf_op args[3]
  1.4 1.4 %copy.11.routes_ref = s32[128,2]{1,0:T(8,128)} copy(s32[128,2]{0,1:T(2,128)} %param.12) | data formatting | bytes 2048 | tf_op args[2]
  2.8 74.6 %shard_map.100 = bf16[128,2048]{1,0:T(8,128)(2,1)} custom-call(s32[2,128]{1,0:T(2,128)} %bitcast.11, s32[128,2]{1,0:T(8,128)} %copy.11.routes_ref, f32[128,2]{1,0:T(8,128)} %copy.12.weights_ref, bf16[128,2048]{1,0:T(8,128)(2,1)} %tokens_ref.1, f32[1,2048]{1,0:T(1,128)} %bitcast.9, f32[1,2048]{1,0:T(1,128)} %bitcast.10, bf16[128,256]{1,0:T(8,128)(2,1)} %din_ref.1, ...), custom_call_target="tpu_custom_call" | custom-call | tf_op jit(solution)/shard_map/pallas_call | solution.py:428
  77.4 1.9 %copy.14 = bf16[128,2048]{1,0:T(8,128)(2,1)} copy(bf16[128,2048]{1,0:T(8,128)(2,1)} %shard_map.100) | data formatting | bytes 1048576
where the time goes:
time: 79.5 us; the launch traced here: 79.3 us
  Pallas kernels  74.6 us (94%)
  local copies, waits for them, and re-layouts  4.7 us (6%)
    pallas_call x1, Pallas kernels, shards(): pl.pallas_call(functools.partial(layer_kernel, (n, n1, n2, cap, blocks)),...  74.6 us
    unnamed x3, local copies, waits for them, and re-layouts  4.7 us

commit v1 on v0

--- a/solution.py
+++ b/solution.py
@@ -405,6 +405,622 @@
     each(n2 - 1, lambda i: dense_copy2((spot + 1 + i) % n2, spot).wait_send())
 
 
+LANES = 128
+
+
+def gateway_kernel(
+    sizes,
+    routes_ref,
+    weights_ref,
+    tokens_ref,
+    gain_ref,
+    dgate_ref,
+    din_ref,
+    dout_ref,
+    wg_ref,
+    wu_ref,
+    wd_ref,
+    out_ref,
+    routes_of,
+    weights_of,
+    dense,
+    picks,
+    wanted,
+    columns,
+    buf,
+    recv,
+    xs,
+    hid,
+    unpack_ref,
+    pack_ref,
+    outb,
+    ret,
+    accs,
+    pout,
+    fin,
+    wgs,
+    wus,
+    wds,
+    dn,
+    w_local,
+    w_send,
+    w_recv,
+    meta_send,
+    meta_recv,
+    dense_send,
+    dense_recv,
+    send1,
+    recv1,
+    send2,
+    recv2,
+    fin_send,
+    fin_recv,
+    dn_send,
+    dn_recv,
+):
+    n, n1, n2, cap, blocks = sizes
+    rows, width = tokens_ref.shape
+    half = wg_ref.shape[1]
+    tall = blocks * cap
+    chunk = blocks * LANES
+    chunks = width // chunk
+    near = n // 2
+    group_rows, packed_rows = n2 * cap, n2 * tall
+    me = lax.axis_index("ep")
+    core = lax.axis_index("tp")
+    peer = 1 - core
+    plane, spot = me // n2, me % n2
+    side = plane // 2
+    mine = me % near
+    base = side * near
+    is_gate = (plane + 1) // 2 % 2
+    sibling = plane + 1 - 2 * (plane % 2)
+    gate_plane = 1 + side
+    far_gate = 2 - side
+    gates_end = (plane + 2) % 4
+    on_gate = is_gate == 1
+    on_end = is_gate == 0
+
+    def at(where):
+        return {"ep": where}
+
+    def each(count, act):
+        def step(i, carry):
+            act(i)
+            return carry
+
+        lax.fori_loop(0, count, step, 0)
+
+    def remote(src, dst, send_sem, recv_sem, device):
+        return pltpu.make_async_remote_copy(
+            src_ref=src,
+            dst_ref=dst,
+            send_sem=send_sem,
+            recv_sem=recv_sem,
+            device_id=device,
+            device_id_type=MESH,
+        )
+
+    barrier = pltpu.get_barrier_semaphore()
+
+    def greet(device):
+        pl.semaphore_signal(barrier, inc=1, device_id=device, device_id_type=MESH)
+
+    each(near - 1, lambda i: greet(at(base + (mine + 1 + i) % near)))
+    greet({"tp": peer})
+    greet(at(far_gate * n2 + spot))
+
+    @pl.when(on_gate)
+    def _():
+        greet(at(gates_end * n2 + spot))
+
+    weight_pairs = ((wg_ref, wgs), (wu_ref, wus), (wd_ref, wds))
+    for i, (src, dst) in enumerate(weight_pairs):
+        pltpu.make_async_copy(src, dst.at[0], w_local.at[i]).start()
+
+    @pl.when(core == 0)
+    def _():
+        dn[0, plane, spot] = din_ref[...]
+
+    @pl.when(core == 1)
+    def _():
+        dn[1, plane, spot] = dout_ref[...]
+
+    widened = tokens_ref[...].astype(F32)
+    inv_scale = lax.rsqrt(jnp.mean(widened * widened, axis=1, keepdims=True) + NORM_EPS)
+    normed = (widened * inv_scale * gain_ref[...]).astype(BF16)
+    for c in range(chunks):
+        for j in range(blocks):
+            low = c * chunk + j * LANES
+            dense[0, c, j * rows : (j + 1) * rows, :] = normed[:, low : low + LANES]
+    routes_of[0] = routes_ref[...]
+    weights_of[0] = weights_ref[...]
+
+    def prepare(kind):
+        experts = lax.broadcasted_iota(jnp.int32, (near, rows), 0) + base
+        first, second = routes_of[kind, 0:1, :], routes_of[kind, 1:2, :]
+        takes = (first == experts, second == experts)
+        chosen = takes[0] | takes[1]
+        earlier = (
+            lax.broadcasted_iota(jnp.int32, (rows, rows), 0)
+            < lax.broadcasted_iota(jnp.int32, (rows, rows), 1)
+        )
+        counted = jnp.dot(
+            jnp.where(chosen, 1.0, 0.0).astype(BF16),
+            jnp.where(earlier, 1.0, 0.0).astype(BF16),
+            preferred_element_type=F32,
+        )
+        slots = counted.astype(jnp.int32)
+        keys = jnp.concatenate(
+            [jnp.where(chosen, slots + j * cap, -1) for j in range(blocks)], axis=1
+        )
+        hits = keys[:, None, :] == lax.broadcasted_iota(
+            jnp.int32, (near, tall, blocks * rows), 1
+        )
+        picks[kind] = (
+            jnp.where(hits, 1.0, 0.0).reshape(near * tall, blocks * rows).astype(BF16)
+        )
+        local = lax.broadcasted_iota(jnp.int32, (near, rows), 0) * tall
+        places = [
+            jnp.sum(
+                jnp.where(take, counted + local.astype(F32) + n * tall, 0.0),
+                axis=0,
+                keepdims=True,
+            )
+            - n * tall
+            for take in takes
+        ]
+        stack = jnp.concatenate(
+            places + [weights_of[kind], jnp.zeros((4, rows), F32)], axis=0
+        )
+        turned = jnp.transpose(stack)
+        columns[kind] = turned
+        lanes = lax.broadcasted_iota(jnp.int32, (rows, near * tall), 1)
+        for k in range(2):
+            place = turned[:, k : k + 1].astype(jnp.int32)
+            for j in range(blocks):
+                top = (k * blocks + j) * rows
+                wanted[kind, top : top + rows, :] = jnp.where(
+                    place + j * cap == lanes, 1.0, 0.0
+                ).astype(BF16)
+
+    prepare(0)
+
+    def packed_place(r):
+        return (r // cap) % n2 * tall + r // group_rows * cap + r % cap
+
+    upright = lax.broadcasted_iota(jnp.int32, (packed_rows, packed_rows), 0)
+    across = lax.broadcasted_iota(jnp.int32, (packed_rows, packed_rows), 1)
+    unpack_ref[...] = jnp.where(packed_place(upright) == across, 1.0, 0.0).astype(BF16)
+    pack_ref[...] = jnp.where(packed_place(across) == upright, 1.0, 0.0).astype(BF16)
+    for kind in range(3):
+        accs[kind] = jnp.zeros((rows, width), F32)
+
+    pl.semaphore_wait(barrier, 9 + is_gate + (near - 8))
+
+    def meta_copies():
+        slot = 2 - is_gate
+        device = at(far_gate * n2 + spot)
+        return (
+            remote(routes_ref, routes_of.at[slot], meta_send.at[0], meta_recv.at[0, slot], device),
+            remote(weights_ref, weights_of.at[slot], meta_send.at[1], meta_recv.at[1, slot], device),
+        )
+
+    def dense_copy(c):
+        slot = 2 - is_gate
+        return remote(
+            dense.at[0, c],
+            dense.at[slot, c],
+            dense_send.at[c],
+            dense_recv.at[slot, c],
+            at(far_gate * n2 + spot),
+        )
+
+    def dense_start():
+        for copy in meta_copies():
+            copy.start()
+        each(chunks, lambda c: dense_copy(c).start())
+
+    def meta_wait(slot):
+        device = at(far_gate * n2 + spot)
+        remote(
+            routes_ref, routes_of.at[slot], meta_send.at[0], meta_recv.at[0, slot], device
+        ).wait_recv()
+        remote(
+            weights_ref, weights_of.at[slot], meta_send.at[1], meta_recv.at[1, slot], device
+        ).wait_recv()
+
+    def dense_wait(slot, c):
+        remote(
+            dense.at[0, c],
+            dense.at[slot, c],
+            dense_send.at[c],
+            dense_recv.at[slot, c],
+            at(far_gate * n2 + spot),
+        ).wait_recv()
+
+    def dn_up():
+        block = dn.at[core, plane, spot]
+        return remote(block, block, dn_send.at[0], dn_recv.at[0], at(sibling * n2 + spot))
+
+    def dn_up_wait():
+        block = dn.at[core, sibling, spot]
+        remote(block, block, dn_send.at[0], dn_recv.at[0], at(sibling * n2 + spot)).wait_recv()
+
+    def dn_cross(which):
+        pair = dn.at[core, pl.ds(which * 2, 2), spot]
+        return remote(pair, pair, dn_send.at[1], dn_recv.at[1], at(far_gate * n2 + spot))
+
+    def dn_flat(part, other, slot):
+        pair = dn.at[core, pl.ds(((side + part) % 2) * 2, 2), slot]
+        return remote(
+            pair,
+            pair,
+            dn_send.at[2 + part * n2 + other],
+            dn_recv.at[2 + part * n2 + slot],
+            at(plane * n2 + other),
+        )
+
+    def dn_swap(which):
+        last = 2 + 2 * n2
+        return remote(
+            dn.at[which], dn.at[which], dn_send.at[last], dn_recv.at[last], {"tp": peer}
+        )
+
+    def weight_copy(i):
+        src, dst = weight_pairs[i]
+        return remote(src, dst.at[1], w_send.at[i], w_recv.at[i], {"tp": peer})
+
+    def dispatch(kind, expert, c):
+        late = (kind + 1) // 2
+        group = (1 - late) * ((expert // n2 + plane) % 2) + late * (kind + 1)
+        return remote(
+            buf.at[kind, expert, c],
+            recv.at[group, spot, c],
+            send1.at[kind, expert, c],
+            recv1.at[group, spot, c],
+            at(base + expert),
+        )
+
+    def select(kind, c):
+        found = jnp.dot(picks[kind], dense[kind, c], preferred_element_type=F32)
+        buf[kind, :, c] = found.reshape(near, tall, LANES).astype(BF16)
+        late = (kind + 1) // 2
+
+        def start(i):
+            expert = (mine + n2 + i) % near
+
+            @pl.when(expert != mine)
+            def _():
+                dispatch(kind, expert, c).start()
+
+            @pl.when(expert == mine)
+            def _():
+                recv[late * (kind + 1), spot, c] = buf[kind, mine, c]
+
+        each(near, start)
+
+    @pl.when(on_gate)
+    def _():
+        dense_start()
+
+    @pl.when(on_end)
+    def _():
+        dn_up().start()
+
+    for i in range(3):
+        weight_copy(i).start()
+    each(chunks, lambda c: select(0, c))
+
+    @pl.when(on_end)
+    def _():
+        dense_start()
+
+    @pl.when(on_gate)
+    def _():
+        dn_up_wait()
+        dn_cross(side).start()
+        each(n2 - 1, lambda i: dn_flat(0, (spot + 1 + i) % n2, spot).start())
+
+    def hop(group):
+        late, odd = group // 2, group % 2
+        return (1 - late) * ((1 - odd) * plane + odd * sibling) + late * gate_plane
+
+    def give_back(group, s, c):
+        late, odd = group // 2, group % 2
+        kind = late * (1 + odd)
+        return remote(
+            outb.at[group, s, c],
+            ret.at[kind, mine, c],
+            send2.at[group, s, c],
+            recv2.at[kind, mine, c],
+            at(hop(group) * n2 + s),
+        )
+
+    piece = min(256, half)
+
+    def run_group(group):
+        origin = hop(group) * n2
+        kind = group // 2 * (1 + group % 2)
+        for c in range(chunks):
+
+            def arrive(s):
+                @pl.when(origin + s != me)
+                def _():
+                    remote(
+                        buf.at[0, 0, c],
+                        recv.at[group, s, c],
+                        send1.at[0, 0, c],
+                        recv1.at[group, s, c],
+                        at(origin + s),
+                    ).wait_recv()
+
+            each(n2, arrive)
+            came = recv[group, :, c].reshape(packed_rows, LANES)
+            apart = jnp.dot(unpack_ref[...], came, preferred_element_type=F32)
+            for j in range(blocks):
+                low = c * chunk + j * LANES
+                xs[:, low : low + LANES] = apart[
+                    j * group_rows : (j + 1) * group_rows
+                ].astype(BF16)
+        x = xs[...]
+        for part in range(2):
+            for low in range(0, half, piece):
+                gate_pre = jnp.dot(
+                    x, wgs[part, :, low : low + piece], preferred_element_type=F32
+                )
+                up_pre = jnp.dot(x, wus[part, :, low : low + piece], preferred_element_type=F32)
+                hid[part, :, low : low + piece] = clamped_unit(gate_pre, up_pre)
+        for c in range(chunks):
+            total = jnp.dot(
+                hid[0], wds[0, :, c * chunk : (c + 1) * chunk], preferred_element_type=F32
+            ) + jnp.dot(
+                hid[1], wds[1, :, c * chunk : (c + 1) * chunk], preferred_element_type=F32
+            )
+            stacked = jnp.concatenate(
+                [total[:, j * LANES : (j + 1) * LANES] for j in range(blocks)], axis=0
+            ).astype(BF16)
+            joined = jnp.dot(pack_ref[...], stacked, preferred_element_type=F32)
+            outb[group, :, c] = joined.reshape(n2, tall, LANES).astype(BF16)
+
+            def start(i):
+                s = (spot + 1 + i) % n2
+
+                @pl.when(origin + s != me)
+                def _():
+                    give_back(group, s, c).start()
+
+                @pl.when(origin + s == me)
+                def _():
+                    ret[kind, mine, c] = outb[group, s, c]
+
+            each(n2, start)
+
+    def gather(kind, c):
+        def arrive(i):
+            expert = (mine + 1 + i) % near
+            remote(
+                outb.at[0, 0, c],
+                ret.at[kind, expert, c],
+                send2.at[0, 0, c],
+                recv2.at[kind, expert, c],
+                at(base + expert),
+            ).wait_recv()
+
+        each(near - 1, arrive)
+        back = ret[kind, :, c].reshape(near * tall, LANES)
+        picked = jnp.dot(wanted[kind], back, preferred_element_type=F32)
+        totals = []
+        for j in range(blocks):
+            total = jnp.zeros((rows, LANES), F32)
+            for k in range(2):
+                top = (k * blocks + j) * rows
+                total = total + picked[top : top + rows] * columns[kind, :, 2 + k : 3 + k]
+            totals.append(total)
+        return jnp.concatenate(totals, axis=1)
+
+    def fin_copy(kind, c):
+        where = (kind - 1) * gates_end + (2 - kind) * far_gate
+        return remote(
+            pout.at[kind, c],
+            fin.at[c],
+            fin_send.at[kind, c],
+            fin_recv.at[c],
+            at(where * n2 + spot),
+        )
+
+    def combine(kind, c):
+        span = pl.ds(pl.multiple_of(c * chunk, chunk), chunk)
+        pout[kind, c] = (accs[kind, :, span] + gather(kind, c)).astype(BF16)
+        fin_copy(kind, c).start()
+
+    def run_turn(i):
+        kind = 1 + i // 2
+        part = chunks // 2
+
+        @pl.when(on_gate)
+        def _():
+            @pl.when(i % 2 == 0)
+            def _():
+                meta_wait(kind)
+                prepare(kind)
+
+            def take(m):
+                c = i % 2 * part + m
+                dense_wait(kind, c)
+                select(kind, c)
+
+            each(part, take)
+
+            @pl.when(i == 3)
+            def _():
+                dn_cross(1 - side).wait_recv()
+                each(n2 - 1, lambda m: dn_flat(1, (spot + 1 + m) % n2, spot).start())
+                each(part, lambda c: combine(1, c))
+
+        @pl.when(i == 0)
+        def _():
+            for w, (src, dst) in enumerate(weight_pairs):
+                pltpu.make_async_copy(src, dst.at[0], w_local.at[w]).wait()
+            for w in range(3):
+                weight_copy(w).wait()
+
+        run_group(i)
+
+    each(n1, run_turn)
+
+    @pl.when(on_gate)
+    def _():
+        part = chunks // 2
+        each(chunks - part, lambda c: combine(1, part + c))
+        for p in range(2):
+            each(
+                n2 - 1,
+                lambda m: dn_flat(p, (spot + 1 + m) % n2, (spot + 1 + m) % n2).wait_recv(),
+            )
+        dn_swap(core).start()
+        dn_swap(peer).wait_recv()
+        depth = din_ref.shape[1]
+        for kind in (2, 0):
+            x = jnp.concatenate(
+                [
+                    dense[kind, c, j * rows : (j + 1) * rows, :]
+                    for c in range(chunks)
+                    for j in range(blocks)
+                ],
+                axis=1,
+            )
+            pre = jnp.dot(x, dn[0].reshape(width, depth), preferred_element_type=F32)
+            dense_hidden = jax.nn.silu(pre).astype(BF16)
+            step = width // n1
+            for z in range(n1):
+                branch = lax.dot_general(
+                    dense_hidden,
+                    dn[1, z].reshape(step, depth),
+                    (((1,), (1,)), ((), ())),
+                    preferred_element_type=F32,
+                )
+                accs[kind, :, z * step : (z + 1) * step] = (
+                    jax.nn.sigmoid(dgate_ref[:, z * step : (z + 1) * step]) * branch
+                )
+        each(chunks, lambda c: combine(2, c))
+
+    def own(c):
+        span = pl.ds(pl.multiple_of(c * chunk, chunk), chunk)
+        accs[0, :, span] = accs[0, :, span] + gather(0, c)
+
+    each(chunks, own)
+
+    def finish(c):
+        remote(
+            pout.at[1, c],
+            fin.at[c],
+            fin_send.at[1, c],
+            fin_recv.at[c],
+            at(far_gate * n2 + spot),
+        ).wait_recv()
+        span = pl.ds(pl.multiple_of(c * chunk, chunk), chunk)
+        out_ref[:, span] = (accs[0, :, span] + fin[c].astype(F32)).astype(BF16)
+
+    each(chunks, finish)
+
+    def drain_dispatch(kind):
+        def go(i):
+            each(chunks, lambda c: dispatch(kind, (mine + 1 + i) % near, c).wait_send())
+
+        each(near - 1, go)
+
+    drain_dispatch(0)
+    for copy in meta_copies():
+        copy.wait_send()
+    each(chunks, lambda c: dense_copy(c).wait_send())
+
+    def drain_back(group):
+        def go(s):
+            @pl.when(hop(group) * n2 + s != me)
+            def _():
+                each(chunks, lambda c: give_back(group, s, c).wait_send())
+
+        each(n2, go)
+
+    each(n1, drain_back)
+
+    @pl.when(on_end)
+    def _():
+        dn_up().wait_send()
+
+    @pl.when(on_gate)
+    def _():
+        for kind in (1, 2):
+            drain_dispatch(kind)
+            each(chunks, lambda c: fin_copy(kind, c).wait_send())
+        dn_cross(side).wait_send()
+        for p in range(2):
+            each(n2 - 1, lambda m: dn_flat(p, (spot + 1 + m) % n2, spot).wait_send())
+        dn_swap(core).wait_send()
+
+
+def gateway_call(sizes, operands):
+    n, n1, n2, cap, blocks = sizes
+    tokens, dense_in, w_gate = operands[2], operands[5], operands[7]
+    rows, width = tokens.shape
+    half, depth = w_gate.shape[1], dense_in.shape[1]
+    tall, near = blocks * cap, n // 2
+    chunk = blocks * LANES
+    chunks = width // chunk
+    packed = n2 * tall
+    vmem = pl.BlockSpec(memory_space=pltpu.VMEM)
+    anywhere = pl.BlockSpec(memory_space=pl.ANY)
+    dma = pltpu.SemaphoreType.DMA
+    return pl.pallas_call(
+        functools.partial(gateway_kernel, sizes),
+        out_shape=jax.ShapeDtypeStruct((rows, width), BF16),
+        in_specs=[vmem] * 7 + [anywhere] * 3,
+        out_specs=vmem,
+        scratch_shapes=[
+            pltpu.VMEM((3, 2, rows), jnp.int32),
+            pltpu.VMEM((3, 2, rows), F32),
+            pltpu.VMEM((3, chunks, blocks * rows, LANES), BF16),
+            pltpu.VMEM((3, near * tall, blocks * rows), BF16),
+            pltpu.VMEM((3, 2 * blocks * rows, near * tall), BF16),
+            pltpu.VMEM((3, rows, 8), F32),
+            pltpu.VMEM((3, near, chunks, tall, LANES), BF16),
+            pltpu.VMEM((n1, n2, chunks, tall, LANES), BF16),
+            pltpu.VMEM((n2 * cap, width), BF16),
+            pltpu.VMEM((2, n2 * cap, half), BF16),
+            pltpu.VMEM((packed, packed), BF16),
+            pltpu.VMEM((packed, packed), BF16),
+            pltpu.VMEM((n1, n2, chunks, tall, LANES), BF16),
+            pltpu.VMEM((3, near, chunks, tall, LANES), BF16),
+            pltpu.VMEM((3, rows, width), F32),
+            pltpu.VMEM((3, chunks, rows, chunk), BF16),
+            pltpu.VMEM((chunks, rows, chunk), BF16),
+            pltpu.VMEM((2, width, half), BF16),
+            pltpu.VMEM((2, width, half), BF16),
+            pltpu.VMEM((2, half, width), BF16),
+            pltpu.VMEM((2, n1, n2, width // n, depth), BF16),
+            dma((3,)),
+            dma((3,)),
+            dma((3,)),
+            dma((2,)),
+            dma((2, 3)),
+            dma((chunks,)),
+            dma((3, chunks)),
+            dma((3, near, chunks)),
+            dma((n1, n2, chunks)),
+            dma((n1, n2, chunks)),
+            dma((3, near, chunks)),
+            dma((3, chunks)),
+            dma((chunks,)),
+            dma((3 + 2 * n2,)),
+            dma((3 + 2 * n2,)),
+        ],
+        compiler_params=pltpu.CompilerParams(
+            collective_id=0, has_side_effects=True, vmem_limit_bytes=60 * 1024 * 1024
+        ),
+    )(*operands)
+
+
 def shards(
     tokens, norm_gain, routes, route_weights, w_gate, w_up, w_down, dense_in, dense_out, dense_gate
 ):
@@ -421,6 +1037,22 @@
     n1 = n // n2
     half = w_gate.shape[2]
     depth = dense_in.shape[1]
+    if n1 == 4 and n2 == 4 and width % (2 * blocks * LANES) == 0 and width % n == 0:
+        return gateway_call(
+            (n, n1, n2, cap, blocks),
+            (
+                routes.T,
+                route_weights.T,
+                tokens,
+                norm_gain.reshape(1, width),
+                dense_gate.reshape(1, width),
+                dense_in,
+                dense_out,
+                w_gate[0],
+                w_up[0],
+                w_down[0],
+            ),
+        )
     vmem = pl.BlockSpec(memory_space=pltpu.VMEM)
     anywhere = pl.BlockSpec(memory_space=pl.ANY)
     dma = pltpu.SemaphoreType.DMA

time: 79.5 us -> 83.3 us (1.048)
  the two profiles are of different devices: /device:TPU:9 before, /device:TPU:0 now
where the time goes in v1:
time: 83.3 us; the launch traced here: 81.8 us
  Pallas kernels  79.9 us (96%)
  local copies, waits for them, and re-layouts  1.88 us (2%)
    pallas_call x1, Pallas kernels, gateway_call(): pl.pallas_call(functools.partial(gateway_kernel, sizes), out_shape=jax.Sh...  79.9 us
    unnamed x1, local copies, waits for them, and re-layouts  1.88 us

profile of v1, /device:TPU:0, one launch (start us, length us, event | category | flops | bytes accessed | tf_op | source)
XLA Modules:
  0.0 81.8 jit_solution(4024298332083854687)
XLA Ops:
  0.0 79.9 %shard_map.100 = bf16[128,2048]{1,0:T(8,128)(2,1)} custom-call(s32[2,128]{1,0:T(2,128)} %bitcast.12, f32[2,128]{1,0:T(2,128)} %bitcast.13, bf16[128,2048]{1,0:T(8,128)(2,1)} %tokens_ref.1, f32[1,2048]{1,0:T(1,128)} %bitcast.10, f32[1,2048]{1,0:T(1,128)} %bitcast.11, bf16[128,256]{1,0:T(8,128)(2,1)} %din_ref.1, bf16[128,256]{1,0:T(8,128)(2,1)} %dout_ref.1, ...), custom_call_target="tpu_custom_call" | custom-call | tf_op jit(solution)/shard_map/pallas_call | solution.py:975
  80.0 1.9 %copy.12 = bf16[128,2048]{1,0:T(8,128)(2,1)} copy(bf16[128,2048]{1,0:T(8,128)(2,1)} %shard_map.100) | data formatting | bytes 1048576

commit v2 on v1

--- a/solution.py
+++ b/solution.py
@@ -435,6 +435,7 @@
     pack_ref,
     outb,
     ret,
+    relay,
     accs,
     pout,
     fin,
@@ -457,6 +458,9 @@
     fin_recv,
     dn_send,
     dn_recv,
+    relay_send,
+    relay_recv,
+    clear,
 ):
     n, n1, n2, cap, blocks = sizes
     rows, width = tokens_ref.shape
@@ -477,7 +481,7 @@
     sibling = plane + 1 - 2 * (plane % 2)
     gate_plane = 1 + side
     far_gate = 2 - side
-    gates_end = (plane + 2) % 4
+    far_end = 3 - 3 * side
     on_gate = is_gate == 1
     on_end = is_gate == 0
 
@@ -512,7 +516,7 @@
 
     @pl.when(on_gate)
     def _():
-        greet(at(gates_end * n2 + spot))
+        greet(at(far_end * n2 + spot))
 
     weight_pairs = ((wg_ref, wgs), (wu_ref, wus), (wd_ref, wds))
     for i, (src, dst) in enumerate(weight_pairs):
@@ -526,13 +530,14 @@
     def _():
         dn[1, plane, spot] = dout_ref[...]
 
-    widened = tokens_ref[...].astype(F32)
-    inv_scale = lax.rsqrt(jnp.mean(widened * widened, axis=1, keepdims=True) + NORM_EPS)
-    normed = (widened * inv_scale * gain_ref[...]).astype(BF16)
-    for c in range(chunks):
-        for j in range(blocks):
-            low = c * chunk + j * LANES
-            dense[0, c, j * rows : (j + 1) * rows, :] = normed[:, low : low + LANES]
+    with jax.named_scope("norm"):
+        widened = tokens_ref[...].astype(F32)
+        inv_scale = lax.rsqrt(jnp.mean(widened * widened, axis=1, keepdims=True) + NORM_EPS)
+        normed = (widened * inv_scale * gain_ref[...]).astype(BF16)
+        for c in range(chunks):
+            for j in range(blocks):
+                low = c * chunk + j * LANES
+                dense[0, c, j * rows : (j + 1) * rows, :] = normed[:, low : low + LANES]
     routes_of[0] = routes_ref[...]
     weights_of[0] = weights_ref[...]
 
@@ -584,7 +589,8 @@
                     place + j * cap == lanes, 1.0, 0.0
                 ).astype(BF16)
 
-    prepare(0)
+    with jax.named_scope("prepare0"):
+        prepare(0)
 
     def packed_place(r):
         return (r // cap) % n2 * tall + r // group_rows * cap + r % cap
@@ -593,76 +599,79 @@
     across = lax.broadcasted_iota(jnp.int32, (packed_rows, packed_rows), 1)
     unpack_ref[...] = jnp.where(packed_place(upright) == across, 1.0, 0.0).astype(BF16)
     pack_ref[...] = jnp.where(packed_place(across) == upright, 1.0, 0.0).astype(BF16)
-    for kind in range(3):
-        accs[kind] = jnp.zeros((rows, width), F32)
-
-    pl.semaphore_wait(barrier, 9 + is_gate + (near - 8))
 
     def meta_copies():
         slot = 2 - is_gate
         device = at(far_gate * n2 + spot)
         return (
-            remote(routes_ref, routes_of.at[slot], meta_send.at[0], meta_recv.at[0, slot], device),
-            remote(weights_ref, weights_of.at[slot], meta_send.at[1], meta_recv.at[1, slot], device),
-        )
-
-    def dense_copy(c):
-        slot = 2 - is_gate
+            remote(routes_ref, routes_of.at[slot], meta_send.at[0], meta_recv.at[0, slot - 1], device),
+            remote(weights_ref, weights_of.at[slot], meta_send.at[1], meta_recv.at[1, slot - 1], device),
+        )
+
+    def meta_wait(slot):
+        device = at(far_gate * n2 + spot)
+        remote(
+            routes_ref, routes_of.at[slot], meta_send.at[0], meta_recv.at[0, slot - 1], device
+        ).wait_recv()
+        remote(
+            weights_ref, weights_of.at[slot], meta_send.at[1], meta_recv.at[1, slot - 1], device
+        ).wait_recv()
+
+    def dense_copy(slot, c):
         return remote(
             dense.at[0, c],
             dense.at[slot, c],
-            dense_send.at[c],
-            dense_recv.at[slot, c],
+            dense_send,
+            dense_recv.at[slot - 1, c],
             at(far_gate * n2 + spot),
         )
 
     def dense_start():
-        for copy in meta_copies():
-            copy.start()
-        each(chunks, lambda c: dense_copy(c).start())
-
-    def meta_wait(slot):
-        device = at(far_gate * n2 + spot)
-        remote(
-            routes_ref, routes_of.at[slot], meta_send.at[0], meta_recv.at[0, slot], device
-        ).wait_recv()
-        remote(
-            weights_ref, weights_of.at[slot], meta_send.at[1], meta_recv.at[1, slot], device
-        ).wait_recv()
-
-    def dense_wait(slot, c):
-        remote(
-            dense.at[0, c],
-            dense.at[slot, c],
-            dense_send.at[c],
-            dense_recv.at[slot, c],
-            at(far_gate * n2 + spot),
-        ).wait_recv()
-
-    def dn_up():
-        block = dn.at[core, plane, spot]
-        return remote(block, block, dn_send.at[0], dn_recv.at[0], at(sibling * n2 + spot))
-
-    def dn_up_wait():
-        block = dn.at[core, sibling, spot]
-        remote(block, block, dn_send.at[0], dn_recv.at[0], at(sibling * n2 + spot)).wait_recv()
+        for c in range(chunks):
+            dense_copy(2 - is_gate, c).start()
+
+    def dn_block(which, index, target):
+        block = dn.at[core, which, spot]
+        return remote(
+            block, block, dn_send.at[index], dn_recv.at[index], at(target * n2 + spot)
+        )
+
+    def dn_near(which):
+        return dn_block(which, 0, sibling)
 
     def dn_cross(which):
-        pair = dn.at[core, pl.ds(which * 2, 2), spot]
-        return remote(pair, pair, dn_send.at[1], dn_recv.at[1], at(far_gate * n2 + spot))
-
-    def dn_flat(part, other, slot):
-        pair = dn.at[core, pl.ds(((side + part) % 2) * 2, 2), slot]
+        return dn_block(which, 1, far_gate)
+
+    def dn_far(which):
+        return dn_block(which, 2, far_gate)
+
+    def dn_down(order):
+        return dn_block(far_end if order else far_gate, 3 + order, sibling)
+
+    first_bit, second_bit = 1 + core, 2 - core
+    first_spot = spot + first_bit - 2 * first_bit * (spot // first_bit % 2)
+    second_spot = spot + second_bit - 2 * second_bit * (spot // second_bit % 2)
+
+    def dn_step(step, slot):
+        columns_of = dn.at[core, :, slot]
         return remote(
-            pair,
-            pair,
-            dn_send.at[2 + part * n2 + other],
-            dn_recv.at[2 + part * n2 + slot],
-            at(plane * n2 + other),
-        )
+            columns_of,
+            columns_of,
+            dn_send.at[5 + step],
+            dn_recv.at[5 + step],
+            at(plane * n2 + (second_spot if step else first_spot)),
+        )
+
+    def dn_start(step):
+        dn_step(step, spot).start()
+        if step:
+            dn_step(step, first_spot).start()
+
+    def dn_bytes(step):
+        return dn_step(step, pl.ds(0, 2) if step else 0)
 
     def dn_swap(which):
-        last = 2 + 2 * n2
+        last = 7
         return remote(
             dn.at[which], dn.at[which], dn_send.at[last], dn_recv.at[last], {"tp": peer}
         )
@@ -671,99 +680,84 @@
         src, dst = weight_pairs[i]
         return remote(src, dst.at[1], w_send.at[i], w_recv.at[i], {"tp": peer})
 
-    def dispatch(kind, expert, c):
-        late = (kind + 1) // 2
-        group = (1 - late) * ((expert // n2 + plane) % 2) + late * (kind + 1)
+    spots = [(spot + i) % n2 for i in range(n2)]
+    inner = plane % 2 * n2
+    outer = n2 - inner
+
+    def dispatch(kind, away, i, c):
+        expert = (outer if away else inner) + spots[i]
+        group = kind + 1 if kind else away
         return remote(
-            buf.at[kind, expert, c],
-            recv.at[group, spot, c],
-            send1.at[kind, expert, c],
-            recv1.at[group, spot, c],
+            buf.at[kind, expert] if c is None else buf.at[kind, expert, c],
+            recv.at[group, spot] if c is None else recv.at[group, spot, c],
+            send1.at[kind * 2 + away],
+            recv1.at[group * chunks + (c or 0)],
             at(base + expert),
         )
 
+    def dispatched(kind, away):
+        sent = buf.at[kind, pl.ds(0, n2 - 1 + away)]
+        remote(sent, sent, send1.at[kind * 2 + away], recv1.at[0], at(base + outer)).wait_send()
+
+    others = [(1, i) for i in range(n2)] + [(0, i) for i in range(1, n2)]
+
+    def select_own():
+        everything = jnp.concatenate([dense[0, c] for c in range(chunks)], axis=1)
+        found = jnp.dot(picks[0], everything, preferred_element_type=F32).astype(BF16)
+        for c in range(chunks):
+            buf[0, :, c] = found[:, c * LANES : (c + 1) * LANES].reshape(near, tall, LANES)
+        for away, i in others:
+            dispatch(0, away, i, None).start()
+        recv[0, spot] = buf[0, mine]
+
     def select(kind, c):
-        found = jnp.dot(picks[kind], dense[kind, c], preferred_element_type=F32)
-        buf[kind, :, c] = found.reshape(near, tall, LANES).astype(BF16)
-        late = (kind + 1) // 2
-
-        def start(i):
-            expert = (mine + n2 + i) % near
-
-            @pl.when(expert != mine)
-            def _():
-                dispatch(kind, expert, c).start()
-
-            @pl.when(expert == mine)
-            def _():
-                recv[late * (kind + 1), spot, c] = buf[kind, mine, c]
-
-        each(near, start)
-
-    @pl.when(on_gate)
-    def _():
-        dense_start()
-
-    @pl.when(on_end)
-    def _():
-        dn_up().start()
-
-    for i in range(3):
-        weight_copy(i).start()
-    each(chunks, lambda c: select(0, c))
-
-    @pl.when(on_end)
-    def _():
-        dense_start()
-
-    @pl.when(on_gate)
-    def _():
-        dn_up_wait()
-        dn_cross(side).start()
-        each(n2 - 1, lambda i: dn_flat(0, (spot + 1 + i) % n2, spot).start())
+        with jax.named_scope("densewait"):
+            dense_copy(kind, c).wait_recv()
+        with jax.named_scope("select"):
+            found = jnp.dot(picks[kind], dense[kind, c], preferred_element_type=F32)
+            buf[kind, :, c] = found.reshape(near, tall, LANES).astype(BF16)
+            for away, i in others:
+                dispatch(kind, away, i, c).start()
+            recv[kind + 1, spot, c] = buf[kind, mine, c]
 
     def hop(group):
-        late, odd = group // 2, group % 2
-        return (1 - late) * ((1 - odd) * plane + odd * sibling) + late * gate_plane
-
-    def give_back(group, s, c):
-        late, odd = group // 2, group % 2
-        kind = late * (1 + odd)
+        return (plane, sibling, gate_plane, gate_plane)[group]
+
+    def give_back(group, i, c):
+        s = spots[i]
+        kind = max(group - 1, 0)
         return remote(
-            outb.at[group, s, c],
-            ret.at[kind, mine, c],
-            send2.at[group, s, c],
-            recv2.at[kind, mine, c],
+            outb.at[group, s] if c is None else outb.at[group, s, c],
+            ret.at[kind, mine] if c is None else ret.at[kind, mine, c],
+            send2.at[group],
+            recv2.at[kind * chunks + (c or 0)],
             at(hop(group) * n2 + s),
         )
 
+    def given_back(group, count):
+        sent = outb.at[group, pl.ds(0, count)]
+        remote(sent, sent, send2.at[group], recv2.at[0], at(base + outer)).wait_send()
+
+    def arrived(group, c, count):
+        part = recv.at[group, pl.ds(0, count)]
+        if c is not None:
+            part = recv.at[group, pl.ds(0, count), c]
+        remote(
+            part, part, send1.at[0], recv1.at[group * chunks + (c or 0)], at(base + outer)
+        ).wait_recv()
+
+    def by_role(act):
+        @pl.when(on_end)
+        def _():
+            act(n2)
+
+        @pl.when(on_gate)
+        def _():
+            act(n2 - 1)
+
     piece = min(256, half)
 
-    def run_group(group):
-        origin = hop(group) * n2
-        kind = group // 2 * (1 + group % 2)
-        for c in range(chunks):
-
-            def arrive(s):
-                @pl.when(origin + s != me)
-                def _():
-                    remote(
-                        buf.at[0, 0, c],
-                        recv.at[group, s, c],
-                        send1.at[0, 0, c],
-                        recv1.at[group, s, c],
-                        at(origin + s),
-                    ).wait_recv()
-
-            each(n2, arrive)
-            came = recv[group, :, c].reshape(packed_rows, LANES)
-            apart = jnp.dot(unpack_ref[...], came, preferred_element_type=F32)
-            for j in range(blocks):
-                low = c * chunk + j * LANES
-                xs[:, low : low + LANES] = apart[
-                    j * group_rows : (j + 1) * group_rows
-                ].astype(BF16)
-        x = xs[...]
+    def feed(x):
         for part in range(2):
             for low in range(0, half, piece):
                 gate_pre = jnp.dot(
@@ -771,193 +765,360 @@
                 )
                 up_pre = jnp.dot(x, wus[part, :, low : low + piece], preferred_element_type=F32)
                 hid[part, :, low : low + piece] = clamped_unit(gate_pre, up_pre)
+
+    def down(c):
+        return jnp.dot(
+            hid[0], wds[0, :, c * chunk : (c + 1) * chunk], preferred_element_type=F32
+        ) + jnp.dot(
+            hid[1], wds[1, :, c * chunk : (c + 1) * chunk], preferred_element_type=F32
+        )
+
+    def stack_tiles(total):
+        return jnp.concatenate(
+            [total[:, j * LANES : (j + 1) * LANES] for j in range(blocks)], axis=0
+        )
+
+    def run_near(group):
+        with jax.named_scope("neararrive"):
+            arrived(group, None, n2 - 1 + group)
+        with jax.named_scope("near"):
+            came = jnp.concatenate(
+                [recv[group, :, c].reshape(packed_rows, LANES) for c in range(chunks)], axis=1
+            )
+            apart = jnp.dot(unpack_ref[...], came, preferred_element_type=F32).astype(BF16)
+            for c in range(chunks):
+                for j in range(blocks):
+                    low = c * chunk + j * LANES
+                    xs[:, low : low + LANES] = apart[
+                        j * group_rows : (j + 1) * group_rows, c * LANES : (c + 1) * LANES
+                    ]
+            feed(xs[...])
+            stacked = jnp.concatenate(
+                [stack_tiles(down(c)) for c in range(chunks)], axis=1
+            ).astype(BF16)
+            joined = jnp.dot(pack_ref[...], stacked, preferred_element_type=F32).astype(BF16)
+            for c in range(chunks):
+                outb[group, :, c] = joined[:, c * LANES : (c + 1) * LANES].reshape(
+                    n2, tall, LANES
+                )
+            if group == 0:
+                ret[0, mine] = outb[0, spot]
+
+    def send_near(group, low, high):
+        for i in range(low, high):
+            give_back(group, i, None).start()
+
+    def run_far(group):
         for c in range(chunks):
-            total = jnp.dot(
-                hid[0], wds[0, :, c * chunk : (c + 1) * chunk], preferred_element_type=F32
-            ) + jnp.dot(
-                hid[1], wds[1, :, c * chunk : (c + 1) * chunk], preferred_element_type=F32
-            )
-            stacked = jnp.concatenate(
-                [total[:, j * LANES : (j + 1) * LANES] for j in range(blocks)], axis=0
-            ).astype(BF16)
+            with jax.named_scope("arrive"):
+                by_role(lambda count: arrived(group, c, count))
+            came = recv[group, :, c].reshape(packed_rows, LANES)
+            apart = jnp.dot(unpack_ref[...], came, preferred_element_type=F32).astype(BF16)
+            for j in range(blocks):
+                low = c * chunk + j * LANES
+                xs[:, low : low + LANES] = apart[j * group_rows : (j + 1) * group_rows]
+        with jax.named_scope("feed"):
+            feed(xs[...])
+        for c in range(chunks):
+            stacked = stack_tiles(down(c)).astype(BF16)
             joined = jnp.dot(pack_ref[...], stacked, preferred_element_type=F32)
             outb[group, :, c] = joined.reshape(n2, tall, LANES).astype(BF16)
 
-            def start(i):
-                s = (spot + 1 + i) % n2
-
-                @pl.when(origin + s != me)
-                def _():
-                    give_back(group, s, c).start()
-
-                @pl.when(origin + s == me)
-                def _():
-                    ret[kind, mine, c] = outb[group, s, c]
-
-            each(n2, start)
-
-    def gather(kind, c):
-        def arrive(i):
-            expert = (mine + 1 + i) % near
-            remote(
-                outb.at[0, 0, c],
-                ret.at[kind, expert, c],
-                send2.at[0, 0, c],
-                recv2.at[kind, expert, c],
-                at(base + expert),
-            ).wait_recv()
-
-        each(near - 1, arrive)
-        back = ret[kind, :, c].reshape(near * tall, LANES)
-        picked = jnp.dot(wanted[kind], back, preferred_element_type=F32)
+            @pl.when(on_end)
+            def _():
+                for i in range(1, n2):
+                    pass_on(group, i, c).start()
+                relay[group - 2, spot, c] = outb[group, spot, c]
+
+            @pl.when(on_gate)
+            def _():
+                for i in range(1, n2):
+                    give_back(group, i, c).start()
+                ret[group - 1, mine, c] = outb[group, spot, c]
+
+    def pass_on(group, i, c):
+        s = spots[i]
+        return remote(
+            outb.at[group, s, c],
+            relay.at[group - 2, spot, c],
+            send2.at[group],
+            relay_recv.at[(group - 2) * chunks + c],
+            at(plane * n2 + s),
+        )
+
+    def forward(group, c):
+        return remote(
+            relay.at[group - 2, :, c],
+            ret.at[group - 1, pl.ds(inner, n2), c],
+            relay_send.at[group - 2],
+            recv2.at[(group - 1) * chunks + c],
+            at(sibling * n2 + spot),
+        )
+
+    def run_relay(group):
+        with jax.named_scope("relay"):
+            for c in range(chunks):
+                part = relay.at[group - 2, pl.ds(0, n2 - 1), c]
+                remote(
+                    part,
+                    part,
+                    relay_send.at[0],
+                    relay_recv.at[(group - 2) * chunks + c],
+                    at(base + outer),
+                ).wait_recv()
+                forward(group, c).start()
+
+    def returned(kind, c):
+        part = ret.at[kind, pl.ds(0, near - 1)]
+        if c is not None:
+            part = ret.at[kind, pl.ds(0, near - 1), c]
+        remote(
+            part, part, send2.at[0], recv2.at[kind * chunks + (c or 0)], at(base + outer)
+        ).wait_recv()
+
+    def weigh(kind, picked):
         totals = []
         for j in range(blocks):
-            total = jnp.zeros((rows, LANES), F32)
+            total = jnp.zeros((rows, picked.shape[1]), F32)
             for k in range(2):
                 top = (k * blocks + j) * rows
                 total = total + picked[top : top + rows] * columns[kind, :, 2 + k : 3 + k]
             totals.append(total)
-        return jnp.concatenate(totals, axis=1)
+        return totals
 
     def fin_copy(kind, c):
-        where = (kind - 1) * gates_end + (2 - kind) * far_gate
+        where = far_end if kind == 2 else far_gate
         return remote(
-            pout.at[kind, c],
+            pout.at[kind - 1, c],
             fin.at[c],
-            fin_send.at[kind, c],
+            fin_send.at[kind - 1],
             fin_recv.at[c],
             at(where * n2 + spot),
         )
 
     def combine(kind, c):
-        span = pl.ds(pl.multiple_of(c * chunk, chunk), chunk)
-        pout[kind, c] = (accs[kind, :, span] + gather(kind, c)).astype(BF16)
-        fin_copy(kind, c).start()
-
-    def run_turn(i):
-        kind = 1 + i // 2
-        part = chunks // 2
+        with jax.named_scope("gatherwait"):
+            returned(kind, c)
+        with jax.named_scope("combine"):
+            back = ret[kind, :, c].reshape(near * tall, LANES)
+            picked = jnp.dot(wanted[kind], back, preferred_element_type=F32)
+            total = jnp.concatenate(weigh(kind, picked), axis=1)
+            pout[kind - 1, c] = total.astype(BF16)
+            fin_copy(kind, c).start()
+
+    def dense_branch():
+        depth = din_ref.shape[1]
+        x = jnp.concatenate(
+            [
+                dense[0, c, j * rows : (j + 1) * rows, :]
+                for c in range(chunks)
+                for j in range(blocks)
+            ],
+            axis=1,
+        )
+        pre = jnp.dot(x, dn[0].reshape(width, depth), preferred_element_type=F32)
+        dense_hidden = jax.nn.silu(pre).astype(BF16)
+        step = width // n1
+        for z in range(n1):
+            branch = lax.dot_general(
+                dense_hidden,
+                dn[1, z].reshape(step, depth),
+                (((1,), (1,)), ((), ())),
+                preferred_element_type=F32,
+            )
+            accs[:, z * step : (z + 1) * step] = (
+                jax.nn.sigmoid(dgate_ref[:, z * step : (z + 1) * step]) * branch
+            )
+
+    def own():
+        with jax.named_scope("ownwait"):
+            returned(0, None)
+        back = jnp.concatenate(
+            [ret[0, :, c].reshape(near * tall, LANES) for c in range(chunks)], axis=1
+        )
+        picked = jnp.dot(wanted[0], back, preferred_element_type=F32)
+        totals = weigh(0, picked)
+        for c in range(chunks):
+            for j in range(blocks):
+                low = c * chunk + j * LANES
+                accs[:, low : low + LANES] = (
+                    accs[:, low : low + LANES] + totals[j][:, c * LANES : (c + 1) * LANES]
+                )
+
+    with jax.named_scope("barrier"):
+        pl.semaphore_wait(barrier, near + 1 + is_gate)
+    for copy in meta_copies():
+        copy.start()
+
+    @pl.when(on_gate)
+    def _():
+        dn_cross(plane).start()
+
+    dense_start()
+    dn_near(plane).start()
+
+    @pl.when(on_end)
+    def _():
+        dn_far(plane).start()
+
+    for i in range(3):
+        weight_copy(i).start()
+    with jax.named_scope("selectown"):
+        select_own()
+
+    def weights_wait():
+        with jax.named_scope("weightwait"):
+            for i, (src, dst) in enumerate(weight_pairs):
+                pltpu.make_async_copy(src, dst.at[0], w_local.at[i]).wait()
+            for i in range(3):
+                weight_copy(i).wait()
+
+    def prepare_for(kind):
+        with jax.named_scope("prepare"):
+            meta_wait(kind)
+            prepare(kind)
+
+    part = chunks // 2
+
+    def step_wait():
+        with jax.named_scope("stepwait"):
+            dn_bytes(0).wait_recv()
+
+    @pl.when(on_gate)
+    def _():
+        prepare_for(2)
+        for c in range(part):
+            select(2, c)
+        weights_wait()
+        run_near(0)
+        for c in range(part, chunks):
+            select(2, c)
+        prepare_for(1)
+        select(1, 0)
+        with jax.named_scope("upwait"):
+            dn_cross(far_gate).wait_recv()
+        dn_down(0).start()
+        select(1, 1)
+        with jax.named_scope("upwait"):
+            dn_far(far_end).wait_recv()
+            dn_near(sibling).wait_recv()
+        dn_down(1).start()
+        dn_start(0)
+
+    @pl.when(on_end)
+    def _():
+        weights_wait()
+        run_near(0)
+        send_near(0, 1, n2)
+        run_near(1)
+
+    with jax.named_scope("farC"):
+        run_far(3)
+
+    @pl.when(on_end)
+    def _():
+        run_relay(3)
+        send_near(1, 0, part)
+        with jax.named_scope("upwait"):
+            dn_near(sibling).wait_recv()
+            for order in range(2):
+                dn_down(order).wait_recv()
+        dn_start(0)
+
+    @pl.when(on_gate)
+    def _():
+        for c in range(part, chunks):
+            select(1, c)
+        step_wait()
+        dn_start(1)
+        run_near(1)
+        with jax.named_scope("sentwait"):
+            dispatched(1, 1)
+            pl.semaphore_signal(
+                clear, inc=1, device_id=at(far_gate * n2 + spot), device_id_type=MESH
+            )
+            pl.semaphore_wait(clear, 1)
+        for c in range(chunks):
+            combine(2, c)
+
+    with jax.named_scope("farB"):
+        run_far(2)
+
+    @pl.when(on_gate)
+    def _():
+        send_near(0, 1, n2)
+        send_near(1, 0, n2)
+        for c in range(chunks):
+            combine(1, c)
+
+    @pl.when(on_end)
+    def _():
+        run_relay(2)
+        send_near(1, part, n2)
+        step_wait()
+        dn_start(1)
+
+    with jax.named_scope("dnwait"):
+        dn_bytes(1).wait_recv()
+        dn_swap(core).start()
+        dn_swap(peer).wait_recv()
+    with jax.named_scope("densebranch"):
+        dense_branch()
+    with jax.named_scope("own"):
+        own()
+
+    with jax.named_scope("drain"):
+        for away in range(2):
+            dispatched(0, away)
+        for copy in meta_copies():
+            copy.wait_send()
+        remote(
+            dense.at[0], dense.at[0], dense_send, dense_recv.at[0, 0], at(base + outer)
+        ).wait_send()
+        for group in range(2):
+            given_back(group, n2 - 1 + group)
+        for group in range(2, n1):
+            given_back(group, n2 - 1)
+        dn_near(plane).wait_send()
+        for step in range(2):
+            dn_bytes(step).wait_send()
+        dn_swap(core).wait_send()
+
+        @pl.when(on_end)
+        def _():
+            dn_far(plane).wait_send()
+            for group in (0, 1):
+                remote(
+                    relay.at[group],
+                    relay.at[group],
+                    relay_send.at[group],
+                    relay_recv.at[0],
+                    at(base + outer),
+                ).wait_send()
 
         @pl.when(on_gate)
         def _():
-            @pl.when(i % 2 == 0)
-            def _():
-                meta_wait(kind)
-                prepare(kind)
-
-            def take(m):
-                c = i % 2 * part + m
-                dense_wait(kind, c)
-                select(kind, c)
-
-            each(part, take)
-
-            @pl.when(i == 3)
-            def _():
-                dn_cross(1 - side).wait_recv()
-                each(n2 - 1, lambda m: dn_flat(1, (spot + 1 + m) % n2, spot).start())
-                each(part, lambda c: combine(1, c))
-
-        @pl.when(i == 0)
-        def _():
-            for w, (src, dst) in enumerate(weight_pairs):
-                pltpu.make_async_copy(src, dst.at[0], w_local.at[w]).wait()
-            for w in range(3):
-                weight_copy(w).wait()
-
-        run_group(i)
-
-    each(n1, run_turn)
+            for away in range(2):
+                dispatched(2, away)
+            dispatched(1, 0)
+            dn_cross(plane).wait_send()
+            for order in range(2):
+                dn_down(order).wait_send()
+
+    with jax.named_scope("finish"):
+        for c in range(chunks):
+            with jax.named_scope("finwait"):
+                fin_copy(1, c).wait_recv()
+            span = slice(c * chunk, (c + 1) * chunk)
+            out_ref[:, span] = (accs[:, span] + fin[c].astype(F32)).astype(BF16)
 
     @pl.when(on_gate)
     def _():
-        part = chunks // 2
-        each(chunks - part, lambda c: combine(1, part + c))
-        for p in range(2):
-            each(
-                n2 - 1,
-                lambda m: dn_flat(p, (spot + 1 + m) % n2, (spot + 1 + m) % n2).wait_recv(),
-            )
-        dn_swap(core).start()
-        dn_swap(peer).wait_recv()
-        depth = din_ref.shape[1]
-        for kind in (2, 0):
-            x = jnp.concatenate(
-                [
-                    dense[kind, c, j * rows : (j + 1) * rows, :]
-                    for c in range(chunks)
-                    for j in range(blocks)
-                ],
-                axis=1,
-            )
-            pre = jnp.dot(x, dn[0].reshape(width, depth), preferred_element_type=F32)
-            dense_hidden = jax.nn.silu(pre).astype(BF16)
-            step = width // n1
-            for z in range(n1):
-                branch = lax.dot_general(
-                    dense_hidden,
-                    dn[1, z].reshape(step, depth),
-                    (((1,), (1,)), ((), ())),
-                    preferred_element_type=F32,
-                )
-                accs[kind, :, z * step : (z + 1) * step] = (
-                    jax.nn.sigmoid(dgate_ref[:, z * step : (z + 1) * step]) * branch
-                )
-        each(chunks, lambda c: combine(2, c))
-
-    def own(c):
-        span = pl.ds(pl.multiple_of(c * chunk, chunk), chunk)
-        accs[0, :, span] = accs[0, :, span] + gather(0, c)
-
-    each(chunks, own)
-
-    def finish(c):
-        remote(
-            pout.at[1, c],
-            fin.at[c],
-            fin_send.at[1, c],
-            fin_recv.at[c],
-            at(far_gate * n2 + spot),
-        ).wait_recv()
-        span = pl.ds(pl.multiple_of(c * chunk, chunk), chunk)
-        out_ref[:, span] = (accs[0, :, span] + fin[c].astype(F32)).astype(BF16)
-
-    each(chunks, finish)
-
-    def drain_dispatch(kind):
-        def go(i):
-            each(chunks, lambda c: dispatch(kind, (mine + 1 + i) % near, c).wait_send())
-
-        each(near - 1, go)
-
-    drain_dispatch(0)
-    for copy in meta_copies():
-        copy.wait_send()
-    each(chunks, lambda c: dense_copy(c).wait_send())
-
-    def drain_back(group):
-        def go(s):
-            @pl.when(hop(group) * n2 + s != me)
-            def _():
-                each(chunks, lambda c: give_back(group, s, c).wait_send())
-
-        each(n2, go)
-
-    each(n1, drain_back)
-
-    @pl.when(on_end)
-    def _():
-        dn_up().wait_send()
-
-    @pl.when(on_gate)
-    def _():
         for kind in (1, 2):
-            drain_dispatch(kind)
-            each(chunks, lambda c: fin_copy(kind, c).wait_send())
-        dn_cross(side).wait_send()
-        for p in range(2):
-            each(n2 - 1, lambda m: dn_flat(p, (spot + 1 + m) % n2, spot).wait_send())
-        dn_swap(core).wait_send()
+            sent = pout.at[kind - 1]
+            remote(
+                sent, sent, fin_send.at[kind - 1], fin_recv.at[0], at(base + outer)
+            ).wait_send()
 
 
 def gateway_call(sizes, operands):
@@ -992,8 +1153,9 @@
             pltpu.VMEM((packed, packed), BF16),
             pltpu.VMEM((n1, n2, chunks, tall, LANES), BF16),
             pltpu.VMEM((3, near, chunks, tall, LANES), BF16),
-            pltpu.VMEM((3, rows, width), F32),
-            pltpu.VMEM((3, chunks, rows, chunk), BF16),
+            pltpu.VMEM((2, n2, chunks, tall, LANES), BF16),
+            pltpu.VMEM((rows, width), F32),
+            pltpu.VMEM((2, chunks, rows, chunk), BF16),
             pltpu.VMEM((chunks, rows, chunk), BF16),
             pltpu.VMEM((2, width, half), BF16),
             pltpu.VMEM((2, width, half), BF16),
@@ -1003,17 +1165,20 @@
             dma((3,)),
             dma((3,)),
             dma((2,)),
-            dma((2, 3)),
+            dma((2, 2)),
+            dma,
+            dma((2, chunks)),
+            dma((6,)),
+            dma((n1 * chunks,)),
+            dma((n1,)),
+            dma((3 * chunks,)),
+            dma((2,)),
             dma((chunks,)),
-            dma((3, chunks)),
-            dma((3, near, chunks)),
-            dma((n1, n2, chunks)),
-            dma((n1, n2, chunks)),
-            dma((3, near, chunks)),
-            dma((3, chunks)),
-            dma((chunks,)),
-            dma((3 + 2 * n2,)),
-            dma((3 + 2 * n2,)),
+            dma((8,)),
+            dma((8,)),
+            dma((2,)),
+            dma((2 * chunks,)),
+            pltpu.SemaphoreType.REGULAR,
         ],
         compiler_params=pltpu.CompilerParams(
             collective_id=0, has_side_effects=True, vmem_limit_bytes=60 * 1024 * 1024

time: 83.3 us -> 67.9 us (0.82); the launches traced: 81.8 us -> 67.8 us
  Pallas kernels: 79.9 us -> 65.9 us
    pallas_call x1, Pallas kernels: 79.9 us -> 65.9 us  [gateway_call(): pl.pallas_call(functools.partial(gateway_kernel, sizes), out_shape=jax.Sh...]
where the time goes in v2:
time: 67.9 us; the launch traced here: 67.8 us
  Pallas kernels  65.9 us (97%)
  local copies, waits for them, and re-layouts  1.88 us (3%)
    pallas_call x1, Pallas kernels, gateway_call(): pl.pallas_call(functools.partial(gateway_kernel, sizes), out_shape=jax.Sh...  65.9 us
    unnamed x1, local copies, waits for them, and re-layouts  1.88 us

profile of v2, /device:TPU:0, one launch (start us, length us, event | category | flops | bytes accessed | tf_op | source)
XLA Modules:
  0.0 67.8 jit_solution(3085124453069862897)
XLA Ops:
  0.0 65.9 %shard_map.100 = bf16[128,2048]{1,0:T(8,128)(2,1)} custom-call(s32[2,128]{1,0:T(2,128)} %bitcast.12, f32[2,128]{1,0:T(2,128)} %bitcast.13, bf16[128,2048]{1,0:T(8,128)(2,1)} %tokens_ref.1, f32[1,2048]{1,0:T(1,128)} %bitcast.10, f32[1,2048]{1,0:T(1,128)} %bitcast.11, bf16[128,256]{1,0:T(8,128)(2,1)} %din_ref.1, bf16[128,256]{1,0:T(8,128)(2,1)} %dout_ref.1, ...), custom_call_target="tpu_custom_call" | custom-call | tf_op jit(solution)/shard_map/pallas_call | solution.py:1136
  65.9 1.9 %copy.12 = bf16[128,2048]{1,0:T(8,128)(2,1)} copy(bf16[128,2048]{1,0:T(8,128)(2,1)} %shard_map.100) | data formatting | bytes 1048576

commit v3 on v2

--- a/solution.py
+++ b/solution.py
@@ -406,6 +406,7 @@
 
 
 LANES = 128
+CHUNKS = 4
 
 
 def gateway_kernel(
@@ -421,6 +422,9 @@
     wu_ref,
     wd_ref,
     out_ref,
+    tokens_in,
+    gain_in,
+    dgate_in,
     routes_of,
     weights_of,
     dense,
@@ -431,14 +435,13 @@
     recv,
     xs,
     hid,
-    unpack_ref,
-    pack_ref,
     outb,
     ret,
     relay,
     accs,
     pout,
     fin,
+    through,
     wgs,
     wus,
     wds,
@@ -460,16 +463,17 @@
     dn_recv,
     relay_send,
     relay_recv,
-    clear,
+    through_send,
+    through_recv,
+    inputs,
 ):
-    n, n1, n2, cap, blocks = sizes
+    n, n1, n2, tall = sizes
     rows, width = tokens_ref.shape
     half = wg_ref.shape[1]
-    tall = blocks * cap
-    chunk = blocks * LANES
-    chunks = width // chunk
+    chunks = CHUNKS
+    chunk = width // chunks
     near = n // 2
-    group_rows, packed_rows = n2 * cap, n2 * tall
+    group_rows = n2 * tall
     me = lax.axis_index("ep")
     core = lax.axis_index("tp")
     peer = 1 - core
@@ -506,6 +510,19 @@
         )
 
     barrier = pltpu.get_barrier_semaphore()
+    small_pairs = (
+        (tokens_ref, tokens_in),
+        (gain_ref, gain_in),
+        (routes_ref, routes_of.at[0]),
+        (weights_ref, weights_of.at[0]),
+        (dgate_ref, dgate_in),
+    )
+    small_copies = [
+        pltpu.make_async_copy(src, dst, inputs.at[i])
+        for i, (src, dst) in enumerate(small_pairs)
+    ]
+    for copy in small_copies:
+        copy.start()
 
     def greet(device):
         pl.semaphore_signal(barrier, inc=1, device_id=device, device_id_type=MESH)
@@ -518,28 +535,30 @@
     def _():
         greet(at(far_end * n2 + spot))
 
+    def block_copy(which):
+        return pltpu.make_async_copy(
+            (din_ref, dout_ref)[which], dn.at[which, plane, spot], inputs.at[5]
+        )
+
+    for which in range(2):
+
+        @pl.when(core == which)
+        def _():
+            block_copy(which).start()
+
+    block_copy(0).wait()
+    for copy in small_copies:
+        copy.wait()
     weight_pairs = ((wg_ref, wgs), (wu_ref, wus), (wd_ref, wds))
     for i, (src, dst) in enumerate(weight_pairs):
         pltpu.make_async_copy(src, dst.at[0], w_local.at[i]).start()
 
-    @pl.when(core == 0)
-    def _():
-        dn[0, plane, spot] = din_ref[...]
-
-    @pl.when(core == 1)
-    def _():
-        dn[1, plane, spot] = dout_ref[...]
-
     with jax.named_scope("norm"):
-        widened = tokens_ref[...].astype(F32)
+        widened = tokens_in[...].astype(F32)
         inv_scale = lax.rsqrt(jnp.mean(widened * widened, axis=1, keepdims=True) + NORM_EPS)
-        normed = (widened * inv_scale * gain_ref[...]).astype(BF16)
+        normed = (widened * inv_scale * gain_in[...]).astype(BF16)
         for c in range(chunks):
-            for j in range(blocks):
-                low = c * chunk + j * LANES
-                dense[0, c, j * rows : (j + 1) * rows, :] = normed[:, low : low + LANES]
-    routes_of[0] = routes_ref[...]
-    weights_of[0] = weights_ref[...]
+            dense[0, c] = normed[:, c * chunk : (c + 1) * chunk]
 
     def prepare(kind):
         experts = lax.broadcasted_iota(jnp.int32, (near, rows), 0) + base
@@ -555,16 +574,9 @@
             jnp.where(earlier, 1.0, 0.0).astype(BF16),
             preferred_element_type=F32,
         )
-        slots = counted.astype(jnp.int32)
-        keys = jnp.concatenate(
-            [jnp.where(chosen, slots + j * cap, -1) for j in range(blocks)], axis=1
-        )
-        hits = keys[:, None, :] == lax.broadcasted_iota(
-            jnp.int32, (near, tall, blocks * rows), 1
-        )
-        picks[kind] = (
-            jnp.where(hits, 1.0, 0.0).reshape(near * tall, blocks * rows).astype(BF16)
-        )
+        keys = jnp.where(chosen, counted.astype(jnp.int32), -1)
+        hits = keys[:, None, :] == lax.broadcasted_iota(jnp.int32, (near, tall, rows), 1)
+        picks[kind] = jnp.where(hits, 1.0, 0.0).reshape(near * tall, rows).astype(BF16)
         local = lax.broadcasted_iota(jnp.int32, (near, rows), 0) * tall
         places = [
             jnp.sum(
@@ -583,38 +595,28 @@
         lanes = lax.broadcasted_iota(jnp.int32, (rows, near * tall), 1)
         for k in range(2):
             place = turned[:, k : k + 1].astype(jnp.int32)
-            for j in range(blocks):
-                top = (k * blocks + j) * rows
-                wanted[kind, top : top + rows, :] = jnp.where(
-                    place + j * cap == lanes, 1.0, 0.0
-                ).astype(BF16)
+            wanted[kind, k * rows : (k + 1) * rows, :] = jnp.where(
+                place == lanes, 1.0, 0.0
+            ).astype(BF16)
 
     with jax.named_scope("prepare0"):
         prepare(0)
-
-    def packed_place(r):
-        return (r // cap) % n2 * tall + r // group_rows * cap + r % cap
-
-    upright = lax.broadcasted_iota(jnp.int32, (packed_rows, packed_rows), 0)
-    across = lax.broadcasted_iota(jnp.int32, (packed_rows, packed_rows), 1)
-    unpack_ref[...] = jnp.where(packed_place(upright) == across, 1.0, 0.0).astype(BF16)
-    pack_ref[...] = jnp.where(packed_place(across) == upright, 1.0, 0.0).astype(BF16)
 
     def meta_copies():
         slot = 2 - is_gate
         device = at(far_gate * n2 + spot)
         return (
-            remote(routes_ref, routes_of.at[slot], meta_send.at[0], meta_recv.at[0, slot - 1], device),
-            remote(weights_ref, weights_of.at[slot], meta_send.at[1], meta_recv.at[1, slot - 1], device),
+            remote(routes_of.at[0], routes_of.at[slot], meta_send.at[0], meta_recv.at[0, slot - 1], device),
+            remote(weights_of.at[0], weights_of.at[slot], meta_send.at[1], meta_recv.at[1, slot - 1], device),
         )
 
     def meta_wait(slot):
         device = at(far_gate * n2 + spot)
         remote(
-            routes_ref, routes_of.at[slot], meta_send.at[0], meta_recv.at[0, slot - 1], device
+            routes_of.at[0], routes_of.at[slot], meta_send.at[0], meta_recv.at[0, slot - 1], device
         ).wait_recv()
         remote(
-            weights_ref, weights_of.at[slot], meta_send.at[1], meta_recv.at[1, slot - 1], device
+            weights_of.at[0], weights_of.at[slot], meta_send.at[1], meta_recv.at[1, slot - 1], device
         ).wait_recv()
 
     def dense_copy(slot, c):
@@ -652,26 +654,30 @@
     first_spot = spot + first_bit - 2 * first_bit * (spot // first_bit % 2)
     second_spot = spot + second_bit - 2 * second_bit * (spot // second_bit % 2)
 
-    def dn_step(step, slot):
-        columns_of = dn.at[core, :, slot]
+    def dn_step(part, step, block):
+        index = 5 + 2 * part + step
         return remote(
-            columns_of,
-            columns_of,
-            dn_send.at[5 + step],
-            dn_recv.at[5 + step],
+            block,
+            block,
+            dn_send.at[index],
+            dn_recv.at[index],
             at(plane * n2 + (second_spot if step else first_spot)),
         )
 
-    def dn_start(step):
-        dn_step(step, spot).start()
-        if step:
-            dn_step(step, first_spot).start()
-
-    def dn_bytes(step):
-        return dn_step(step, pl.ds(0, 2) if step else 0)
+    def dn_start(part, step):
+        for slot in (spot, first_spot)[: 1 + step]:
+            if part == 0:
+                dn_step(part, step, dn.at[core, plane, slot]).start()
+            else:
+                dn_step(part, step, dn.at[core, sibling, slot]).start()
+                dn_step(part, step, dn.at[core, pl.ds((1 - side) * 2, 2), slot]).start()
+
+    def dn_bytes(part, step):
+        slots = pl.ds(0, 2) if step else 0
+        return dn_step(part, step, dn.at[core, pl.ds(0, n1 - 1) if part else 0, slots])
 
     def dn_swap(which):
-        last = 7
+        last = 9
         return remote(
             dn.at[which], dn.at[which], dn_send.at[last], dn_recv.at[last], {"tp": peer}
         )
@@ -705,7 +711,7 @@
         everything = jnp.concatenate([dense[0, c] for c in range(chunks)], axis=1)
         found = jnp.dot(picks[0], everything, preferred_element_type=F32).astype(BF16)
         for c in range(chunks):
-            buf[0, :, c] = found[:, c * LANES : (c + 1) * LANES].reshape(near, tall, LANES)
+            buf[0, :, c] = found[:, c * chunk : (c + 1) * chunk].reshape(near, tall, chunk)
         for away, i in others:
             dispatch(0, away, i, None).start()
         recv[0, spot] = buf[0, mine]
@@ -715,7 +721,7 @@
             dense_copy(kind, c).wait_recv()
         with jax.named_scope("select"):
             found = jnp.dot(picks[kind], dense[kind, c], preferred_element_type=F32)
-            buf[kind, :, c] = found.reshape(near, tall, LANES).astype(BF16)
+            buf[kind, :, c] = found.astype(BF16).reshape(near, tall, chunk)
             for away, i in others:
                 dispatch(kind, away, i, c).start()
             recv[kind + 1, spot, c] = buf[kind, mine, c]
@@ -773,34 +779,21 @@
             hid[1], wds[1, :, c * chunk : (c + 1) * chunk], preferred_element_type=F32
         )
 
-    def stack_tiles(total):
-        return jnp.concatenate(
-            [total[:, j * LANES : (j + 1) * LANES] for j in range(blocks)], axis=0
-        )
+    def store_out(group, c):
+        outb[group, :, c] = down(c).astype(BF16).reshape(n2, tall, chunk)
+
+    def take_in(group, c):
+        xs[:, c * chunk : (c + 1) * chunk] = recv[group, :, c].reshape(group_rows, chunk)
 
     def run_near(group):
         with jax.named_scope("neararrive"):
             arrived(group, None, n2 - 1 + group)
         with jax.named_scope("near"):
-            came = jnp.concatenate(
-                [recv[group, :, c].reshape(packed_rows, LANES) for c in range(chunks)], axis=1
-            )
-            apart = jnp.dot(unpack_ref[...], came, preferred_element_type=F32).astype(BF16)
             for c in range(chunks):
-                for j in range(blocks):
-                    low = c * chunk + j * LANES
-                    xs[:, low : low + LANES] = apart[
-                        j * group_rows : (j + 1) * group_rows, c * LANES : (c + 1) * LANES
-                    ]
+                take_in(group, c)
             feed(xs[...])
-            stacked = jnp.concatenate(
-                [stack_tiles(down(c)) for c in range(chunks)], axis=1
-            ).astype(BF16)
-            joined = jnp.dot(pack_ref[...], stacked, preferred_element_type=F32).astype(BF16)
             for c in range(chunks):
-                outb[group, :, c] = joined[:, c * LANES : (c + 1) * LANES].reshape(
-                    n2, tall, LANES
-                )
+                store_out(group, c)
             if group == 0:
                 ret[0, mine] = outb[0, spot]
 
@@ -812,17 +805,11 @@
         for c in range(chunks):
             with jax.named_scope("arrive"):
                 by_role(lambda count: arrived(group, c, count))
-            came = recv[group, :, c].reshape(packed_rows, LANES)
-            apart = jnp.dot(unpack_ref[...], came, preferred_element_type=F32).astype(BF16)
-            for j in range(blocks):
-                low = c * chunk + j * LANES
-                xs[:, low : low + LANES] = apart[j * group_rows : (j + 1) * group_rows]
+            take_in(group, c)
         with jax.named_scope("feed"):
             feed(xs[...])
         for c in range(chunks):
-            stacked = stack_tiles(down(c)).astype(BF16)
-            joined = jnp.dot(pack_ref[...], stacked, preferred_element_type=F32)
-            outb[group, :, c] = joined.reshape(n2, tall, LANES).astype(BF16)
+            store_out(group, c)
 
             @pl.when(on_end)
             def _():
@@ -876,43 +863,47 @@
             part, part, send2.at[0], recv2.at[kind * chunks + (c or 0)], at(base + outer)
         ).wait_recv()
 
-    def weigh(kind, picked):
-        totals = []
-        for j in range(blocks):
-            total = jnp.zeros((rows, picked.shape[1]), F32)
-            for k in range(2):
-                top = (k * blocks + j) * rows
-                total = total + picked[top : top + rows] * columns[kind, :, 2 + k : 3 + k]
-            totals.append(total)
-        return totals
+    def weighed(kind, c):
+        back = ret[kind, :, c].reshape(near * tall, chunk)
+        picked = jnp.dot(wanted[kind], back, preferred_element_type=F32)
+        return (
+            picked[:rows] * columns[kind, :, 2:3] + picked[rows:] * columns[kind, :, 3:4]
+        )
 
     def fin_copy(kind, c):
-        where = far_end if kind == 2 else far_gate
+        target = fin.at[c] if kind == 1 else through.at[c]
+        landing = fin_recv.at[c] if kind == 1 else through_recv.at[c]
         return remote(
             pout.at[kind - 1, c],
-            fin.at[c],
+            target,
             fin_send.at[kind - 1],
-            fin_recv.at[c],
-            at(where * n2 + spot),
-        )
+            landing,
+            at(far_gate * n2 + spot),
+        )
+
+    def pass_through(c):
+        return remote(
+            through.at[c], fin.at[c], through_send, fin_recv.at[c], at(sibling * n2 + spot)
+        )
+
+    def run_through(c):
+        with jax.named_scope("through"):
+            fin_copy(2, c).wait_recv()
+            pass_through(c).start()
 
     def combine(kind, c):
         with jax.named_scope("gatherwait"):
             returned(kind, c)
         with jax.named_scope("combine"):
-            back = ret[kind, :, c].reshape(near * tall, LANES)
-            picked = jnp.dot(wanted[kind], back, preferred_element_type=F32)
-            total = jnp.concatenate(weigh(kind, picked), axis=1)
-            pout[kind - 1, c] = total.astype(BF16)
+            pout[kind - 1, c] = weighed(kind, c).astype(BF16)
             fin_copy(kind, c).start()
 
     def dense_branch():
         depth = din_ref.shape[1]
         x = jnp.concatenate(
             [
-                dense[0, c, j * rows : (j + 1) * rows, :]
+                dense[0, c]
                 for c in range(chunks)
-                for j in range(blocks)
             ],
             axis=1,
         )
@@ -927,23 +918,15 @@
                 preferred_element_type=F32,
             )
             accs[:, z * step : (z + 1) * step] = (
-                jax.nn.sigmoid(dgate_ref[:, z * step : (z + 1) * step]) * branch
+                jax.nn.sigmoid(dgate_in[:, z * step : (z + 1) * step]) * branch
             )
 
     def own():
         with jax.named_scope("ownwait"):
             returned(0, None)
-        back = jnp.concatenate(
-            [ret[0, :, c].reshape(near * tall, LANES) for c in range(chunks)], axis=1
-        )
-        picked = jnp.dot(wanted[0], back, preferred_element_type=F32)
-        totals = weigh(0, picked)
         for c in range(chunks):
-            for j in range(blocks):
-                low = c * chunk + j * LANES
-                accs[:, low : low + LANES] = (
-                    accs[:, low : low + LANES] + totals[j][:, c * LANES : (c + 1) * LANES]
-                )
+            span = slice(c * chunk, (c + 1) * chunk)
+            accs[:, span] = accs[:, span] + weighed(0, c)
 
     with jax.named_scope("barrier"):
         pl.semaphore_wait(barrier, near + 1 + is_gate)
@@ -965,6 +948,7 @@
         weight_copy(i).start()
     with jax.named_scope("selectown"):
         select_own()
+    dn_start(0, 0)
 
     def weights_wait():
         with jax.named_scope("weightwait"):
@@ -980,86 +964,91 @@
 
     part = chunks // 2
 
-    def step_wait():
+    def step_wait(index):
         with jax.named_scope("stepwait"):
-            dn_bytes(0).wait_recv()
+            dn_bytes(index, 0).wait_recv()
 
     @pl.when(on_gate)
     def _():
         prepare_for(2)
-        for c in range(part):
+        select(2, 0)
+        step_wait(0)
+        dn_start(0, 1)
+        for c in range(1, chunks):
             select(2, c)
+        prepare_for(1)
         weights_wait()
         run_near(0)
-        for c in range(part, chunks):
-            select(2, c)
-        prepare_for(1)
+        send_near(0, 1, n2)
         select(1, 0)
         with jax.named_scope("upwait"):
             dn_cross(far_gate).wait_recv()
         dn_down(0).start()
+
+    @pl.when(on_end)
+    def _():
+        step_wait(0)
+        dn_start(0, 1)
+        weights_wait()
+        run_near(0)
+        send_near(0, 1, n2)
+        run_near(1)
+
+    with jax.named_scope("farC"):
+        run_far(3)
+
+    @pl.when(on_end)
+    def _():
+        run_relay(3)
+        send_near(1, 0, 1)
+        with jax.named_scope("upwait"):
+            dn_near(sibling).wait_recv()
+            for order in range(2):
+                dn_down(order).wait_recv()
+        dn_start(1, 0)
+
+    @pl.when(on_gate)
+    def _():
         select(1, 1)
         with jax.named_scope("upwait"):
             dn_far(far_end).wait_recv()
             dn_near(sibling).wait_recv()
         dn_down(1).start()
-        dn_start(0)
+        select(1, 2)
+        run_near(1)
+        select(1, 3)
+        dn_start(1, 0)
+        for c in range(chunks):
+            combine(2, c)
+        send_near(1, 0, part)
+        run_through(0)
+
+    with jax.named_scope("farB"):
+        run_far(2)
+
+    @pl.when(on_gate)
+    def _():
+        step_wait(1)
+        dn_start(1, 1)
+        run_through(1)
+        combine(1, 0)
+        run_through(2)
+        send_near(1, part, n2)
+        combine(1, 1)
+        run_through(3)
+        combine(1, 2)
+        combine(1, 3)
 
     @pl.when(on_end)
     def _():
-        weights_wait()
-        run_near(0)
-        send_near(0, 1, n2)
-        run_near(1)
-
-    with jax.named_scope("farC"):
-        run_far(3)
-
-    @pl.when(on_end)
-    def _():
-        run_relay(3)
-        send_near(1, 0, part)
-        with jax.named_scope("upwait"):
-            dn_near(sibling).wait_recv()
-            for order in range(2):
-                dn_down(order).wait_recv()
-        dn_start(0)
-
-    @pl.when(on_gate)
-    def _():
-        for c in range(part, chunks):
-            select(1, c)
-        step_wait()
-        dn_start(1)
-        run_near(1)
-        with jax.named_scope("sentwait"):
-            dispatched(1, 1)
-            pl.semaphore_signal(
-                clear, inc=1, device_id=at(far_gate * n2 + spot), device_id_type=MESH
-            )
-            pl.semaphore_wait(clear, 1)
-        for c in range(chunks):
-            combine(2, c)
-
-    with jax.named_scope("farB"):
-        run_far(2)
-
-    @pl.when(on_gate)
-    def _():
-        send_near(0, 1, n2)
-        send_near(1, 0, n2)
-        for c in range(chunks):
-            combine(1, c)
-
-    @pl.when(on_end)
-    def _():
+        step_wait(1)
+        dn_start(1, 1)
         run_relay(2)
-        send_near(1, part, n2)
-        step_wait()
-        dn_start(1)
+        send_near(1, 1, n2)
 
     with jax.named_scope("dnwait"):
-        dn_bytes(1).wait_recv()
+        for p in range(2):
+            dn_bytes(p, 1).wait_recv()
         dn_swap(core).start()
         dn_swap(peer).wait_recv()
     with jax.named_scope("densebranch"):
@@ -1080,8 +1069,9 @@
         for group in range(2, n1):
             given_back(group, n2 - 1)
         dn_near(plane).wait_send()
-        for step in range(2):
-            dn_bytes(step).wait_send()
+        for p in range(2):
+            for step in range(2):
+                dn_bytes(p, step).wait_send()
         dn_swap(core).wait_send()
 
         @pl.when(on_end)
@@ -1100,7 +1090,11 @@
         def _():
             for away in range(2):
                 dispatched(2, away)
-            dispatched(1, 0)
+            for away in range(2):
+                dispatched(1, away)
+            remote(
+                through, through, through_send, through_recv.at[0], at(base + outer)
+            ).wait_send()
             dn_cross(plane).wait_send()
             for order in range(2):
                 dn_down(order).wait_send()
@@ -1122,40 +1116,40 @@
 
 
 def gateway_call(sizes, operands):
-    n, n1, n2, cap, blocks = sizes
+    n, n1, n2, tall = sizes
     tokens, dense_in, w_gate = operands[2], operands[5], operands[7]
     rows, width = tokens.shape
     half, depth = w_gate.shape[1], dense_in.shape[1]
-    tall, near = blocks * cap, n // 2
-    chunk = blocks * LANES
-    chunks = width // chunk
-    packed = n2 * tall
+    near, chunks = n // 2, CHUNKS
+    chunk = width // chunks
     vmem = pl.BlockSpec(memory_space=pltpu.VMEM)
-    anywhere = pl.BlockSpec(memory_space=pl.ANY)
+    anywhere = pl.BlockSpec(memory_space=pltpu.HBM)
     dma = pltpu.SemaphoreType.DMA
     return pl.pallas_call(
         functools.partial(gateway_kernel, sizes),
         out_shape=jax.ShapeDtypeStruct((rows, width), BF16),
-        in_specs=[vmem] * 7 + [anywhere] * 3,
+        in_specs=[anywhere] * 10,
         out_specs=vmem,
         scratch_shapes=[
+            pltpu.VMEM((rows, width), BF16),
+            pltpu.VMEM((1, width), F32),
+            pltpu.VMEM((1, width), F32),
             pltpu.VMEM((3, 2, rows), jnp.int32),
             pltpu.VMEM((3, 2, rows), F32),
-            pltpu.VMEM((3, chunks, blocks * rows, LANES), BF16),
-            pltpu.VMEM((3, near * tall, blocks * rows), BF16),
-            pltpu.VMEM((3, 2 * blocks * rows, near * tall), BF16),
+            pltpu.VMEM((3, chunks, rows, chunk), BF16),
+            pltpu.VMEM((3, near * tall, rows), BF16),
+            pltpu.VMEM((3, 2 * rows, near * tall), BF16),
             pltpu.VMEM((3, rows, 8), F32),
-            pltpu.VMEM((3, near, chunks, tall, LANES), BF16),
-            pltpu.VMEM((n1, n2, chunks, tall, LANES), BF16),
-            pltpu.VMEM((n2 * cap, width), BF16),
-            pltpu.VMEM((2, n2 * cap, half), BF16),
-            pltpu.VMEM((packed, packed), BF16),
-            pltpu.VMEM((packed, packed), BF16),
-            pltpu.VMEM((n1, n2, chunks, tall, LANES), BF16),
-            pltpu.VMEM((3, near, chunks, tall, LANES), BF16),
-            pltpu.VMEM((2, n2, chunks, tall, LANES), BF16),
+            pltpu.VMEM((3, near, chunks, tall, chunk), BF16),
+            pltpu.VMEM((n1, n2, chunks, tall, chunk), BF16),
+            pltpu.VMEM((n2 * tall, width), BF16),
+            pltpu.VMEM((2, n2 * tall, half), BF16),
+            pltpu.VMEM((n1, n2, chunks, tall, chunk), BF16),
+            pltpu.VMEM((3, near, chunks, tall, chunk), BF16),
+            pltpu.VMEM((2, n2, chunks, tall, chunk), BF16),
             pltpu.VMEM((rows, width), F32),
             pltpu.VMEM((2, chunks, rows, chunk), BF16),
+            pltpu.VMEM((chunks, rows, chunk), BF16),
             pltpu.VMEM((chunks, rows, chunk), BF16),
             pltpu.VMEM((2, width, half), BF16),
             pltpu.VMEM((2, width, half), BF16),
@@ -1174,11 +1168,13 @@
             dma((3 * chunks,)),
             dma((2,)),
             dma((chunks,)),
-            dma((8,)),
-            dma((8,)),
+            dma((10,)),
+            dma((10,)),
             dma((2,)),
             dma((2 * chunks,)),
-            pltpu.SemaphoreType.REGULAR,
+            dma,
+            dma((chunks,)),
+            dma((6,)),
         ],
         compiler_params=pltpu.CompilerParams(
             collective_id=0, has_side_effects=True, vmem_limit_bytes=60 * 1024 * 1024
@@ -1202,9 +1198,9 @@
     n1 = n // n2
     half = w_gate.shape[2]
     depth = dense_in.shape[1]
-    if n1 == 4 and n2 == 4 and width % (2 * blocks * LANES) == 0 and width % n == 0:
+    if n1 == 4 and n2 == 4 and width % (CHUNKS * LANES) == 0 and width % n == 0:
         return gateway_call(
-            (n, n1, n2, cap, blocks),
+            (n, n1, n2, -(-cap // 8) * 8),
             (
                 routes.T,
                 route_weights.T,

time: 67.9 us -> 65.5 us (0.965)
  Pallas kernels: 65.9 us -> 63.5 us
    pallas_call x1, Pallas kernels: 65.9 us -> 63.5 us  [gateway_call(): pl.pallas_call(functools.partial(gateway_kernel, sizes), out_shape=jax.Sh...]
where the time goes in v3:
time: 65.5 us; the launch traced here: 65.4 us
  Pallas kernels  63.5 us (97%)
  local copies, waits for them, and re-layouts  1.88 us (3%)
    pallas_call x1, Pallas kernels, gateway_call(): pl.pallas_call(functools.partial(gateway_kernel, sizes), out_shape=jax.Sh...  63.5 us
    unnamed x1, local copies, waits for them, and re-layouts  1.88 us

profile of v3, /device:TPU:0, one launch (start us, length us, event | category | flops | bytes accessed | tf_op | source)
XLA Modules:
  0.0 65.4 jit_solution(4668653458533287979)
XLA Ops:
  0.0 63.5 %shard_map.100 = bf16[128,2048]{1,0:T(8,128)(2,1)} custom-call(s32[2,128]{1,0:T(2,128)} %bitcast.12, f32[2,128]{1,0:T(2,128)} %bitcast.13, bf16[128,2048]{1,0:T(8,128)(2,1)} %tokens_ref.1, f32[1,2048]{1,0:T(1,128)} %bitcast.10, f32[1,2048]{1,0:T(1,128)} %bitcast.11, bf16[128,256]{1,0:T(8,128)(2,1)} %din_ref.1, bf16[128,256]{1,0:T(8,128)(2,1)} %dout_ref.1, ...), custom_call_target="tpu_custom_call" | custom-call | tf_op jit(solution)/shard_map/pallas_call | solution.py:1128
  63.5 1.9 %copy.12 = bf16[128,2048]{1,0:T(8,128)(2,1)} copy(bf16[128,2048]{1,0:T(8,128)(2,1)} %shard_map.100) | data formatting | bytes 1048576

commit v4 on v3

--- a/solution.py
+++ b/solution.py
@@ -423,6 +423,7 @@
     wd_ref,
     out_ref,
     tokens_in,
+    mixed,
     gain_in,
     dgate_in,
     routes_of,
@@ -466,6 +467,7 @@
     through_send,
     through_recv,
     inputs,
+    out_sem,
 ):
     n, n1, n2, tall = sizes
     rows, width = tokens_ref.shape
@@ -964,6 +966,12 @@
 
     part = chunks // 2
 
+    def swap_start():
+        with jax.named_scope("swapstart"):
+            for p in range(2):
+                dn_bytes(p, 1).wait_recv()
+        dn_swap(core).start()
+
     def step_wait(index):
         with jax.named_scope("stepwait"):
             dn_bytes(index, 0).wait_recv()
@@ -1017,10 +1025,11 @@
         select(1, 2)
         run_near(1)
         select(1, 3)
+        send_near(1, 0, 1)
         dn_start(1, 0)
         for c in range(chunks):
             combine(2, c)
-        send_near(1, 0, part)
+        send_near(1, 1, part)
         run_through(0)
 
     with jax.named_scope("farB"):
@@ -1031,12 +1040,13 @@
         step_wait(1)
         dn_start(1, 1)
         run_through(1)
+        run_through(2)
+        run_through(3)
+        send_near(1, part, n2)
         combine(1, 0)
-        run_through(2)
-        send_near(1, part, n2)
         combine(1, 1)
-        run_through(3)
         combine(1, 2)
+        swap_start()
         combine(1, 3)
 
     @pl.when(on_end)
@@ -1045,11 +1055,9 @@
         dn_start(1, 1)
         run_relay(2)
         send_near(1, 1, n2)
+        swap_start()
 
     with jax.named_scope("dnwait"):
-        for p in range(2):
-            dn_bytes(p, 1).wait_recv()
-        dn_swap(core).start()
         dn_swap(peer).wait_recv()
     with jax.named_scope("densebranch"):
         dense_branch()
@@ -1104,7 +1112,8 @@
             with jax.named_scope("finwait"):
                 fin_copy(1, c).wait_recv()
             span = slice(c * chunk, (c + 1) * chunk)
-            out_ref[:, span] = (accs[:, span] + fin[c].astype(F32)).astype(BF16)
+            mixed[:, span] = (accs[:, span] + fin[c].astype(F32)).astype(BF16)
+            pltpu.make_async_copy(mixed.at[:, span], out_ref.at[:, span], out_sem).start()
 
     @pl.when(on_gate)
     def _():
@@ -1114,6 +1123,8 @@
                 sent, sent, fin_send.at[kind - 1], fin_recv.at[0], at(base + outer)
             ).wait_send()
 
+    pltpu.make_async_copy(mixed, out_ref, out_sem).wait()
+
 
 def gateway_call(sizes, operands):
     n, n1, n2, tall = sizes
@@ -1122,15 +1133,15 @@
     half, depth = w_gate.shape[1], dense_in.shape[1]
     near, chunks = n // 2, CHUNKS
     chunk = width // chunks
-    vmem = pl.BlockSpec(memory_space=pltpu.VMEM)
     anywhere = pl.BlockSpec(memory_space=pltpu.HBM)
     dma = pltpu.SemaphoreType.DMA
     return pl.pallas_call(
         functools.partial(gateway_kernel, sizes),
         out_shape=jax.ShapeDtypeStruct((rows, width), BF16),
         in_specs=[anywhere] * 10,
-        out_specs=vmem,
+        out_specs=anywhere,
         scratch_shapes=[
+            pltpu.VMEM((rows, width), BF16),
             pltpu.VMEM((rows, width), BF16),
             pltpu.VMEM((1, width), F32),
             pltpu.VMEM((1, width), F32),
@@ -1175,6 +1186,7 @@
             dma,
             dma((chunks,)),
             dma((6,)),
+            dma,
         ],
         compiler_params=pltpu.CompilerParams(
             collective_id=0, has_side_effects=True, vmem_limit_bytes=60 * 1024 * 1024

time: 65.5 us -> 63.7 us (0.973)
  Pallas kernels: 63.5 us -> 61.7 us
    pallas_call x1, Pallas kernels: 63.5 us -> 61.7 us  [gateway_call(): pl.pallas_call(functools.partial(gateway_kernel, sizes), out_shape=jax.Sh...]
where the time goes in v4:
time: 63.7 us; the launch traced here: 63.6 us
  Pallas kernels  61.7 us (97%)
  local copies, waits for them, and re-layouts  1.88 us (3%)
    pallas_call x1, Pallas kernels, gateway_call(): pl.pallas_call(functools.partial(gateway_kernel, sizes), out_shape=jax.Sh...  61.7 us
    unnamed x1, local copies, waits for them, and re-layouts  1.88 us

profile of v4, /device:TPU:0, one launch (start us, length us, event | category | flops | bytes accessed | tf_op | source)
XLA Modules:
  0.0 63.6 jit_solution(16684708995210926289)
XLA Ops:
  0.0 61.7 %shard_map.100 = bf16[128,2048]{1,0:T(8,128)(2,1)} custom-call(s32[2,128]{1,0:T(2,128)} %bitcast.12, f32[2,128]{1,0:T(2,128)} %bitcast.13, bf16[128,2048]{1,0:T(8,128)(2,1)} %tokens_ref.1, f32[1,2048]{1,0:T(1,128)} %bitcast.10, f32[1,2048]{1,0:T(1,128)} %bitcast.11, bf16[128,256]{1,0:T(8,128)(2,1)} %din_ref.1, bf16[128,256]{1,0:T(8,128)(2,1)} %dout_ref.1, ...), custom_call_target="tpu_custom_call" | custom-call | tf_op jit(solution)/shard_map/pallas_call | solution.py:1138
  61.7 1.9 %copy.12 = bf16[128,2048]{1,0:T(8,128)(2,1)} copy(bf16[128,2048]{1,0:T(8,128)(2,1)} %shard_map.100) | data formatting | bytes 1048576

commit v5 on v4

--- a/solution.py
+++ b/solution.py
@@ -923,13 +923,6 @@
                 jax.nn.sigmoid(dgate_in[:, z * step : (z + 1) * step]) * branch
             )
 
-    def own():
-        with jax.named_scope("ownwait"):
-            returned(0, None)
-        for c in range(chunks):
-            span = slice(c * chunk, (c + 1) * chunk)
-            accs[:, span] = accs[:, span] + weighed(0, c)
-
     with jax.named_scope("barrier"):
         pl.semaphore_wait(barrier, near + 1 + is_gate)
     for copy in meta_copies():
@@ -1061,8 +1054,18 @@
         dn_swap(peer).wait_recv()
     with jax.named_scope("densebranch"):
         dense_branch()
-    with jax.named_scope("own"):
-        own()
+    with jax.named_scope("ownwait"):
+        returned(0, None)
+
+    with jax.named_scope("finish"):
+        for c in range(chunks):
+            with jax.named_scope("finwait"):
+                fin_copy(1, c).wait_recv()
+            span = slice(c * chunk, (c + 1) * chunk)
+            mixed[:, span] = (
+                accs[:, span] + weighed(0, c) + fin[c].astype(F32)
+            ).astype(BF16)
+            pltpu.make_async_copy(mixed.at[:, span], out_ref.at[:, span], out_sem).start()
 
     with jax.named_scope("drain"):
         for away in range(2):
@@ -1106,14 +1109,6 @@
             dn_cross(plane).wait_send()
             for order in range(2):
                 dn_down(order).wait_send()
-
-    with jax.named_scope("finish"):
-        for c in range(chunks):
-            with jax.named_scope("finwait"):
-                fin_copy(1, c).wait_recv()
-            span = slice(c * chunk, (c + 1) * chunk)
-            mixed[:, span] = (accs[:, span] + fin[c].astype(F32)).astype(BF16)
-            pltpu.make_async_copy(mixed.at[:, span], out_ref.at[:, span], out_sem).start()
 
     @pl.when(on_gate)
     def _():

time: 63.7 us -> 64 us (level)
  no operation moved by 1% of the time
where the time goes in v5:
time: 64 us; the launch traced here: 63.9 us
  Pallas kernels  62 us (97%)
  local copies, waits for them, and re-layouts  1.88 us (3%)
    pallas_call x1, Pallas kernels, gateway_call(): pl.pallas_call(functools.partial(gateway_kernel, sizes), out_shape=jax.Sh...  62 us
    unnamed x1, local copies, waits for them, and re-layouts  1.88 us

profile of v5, /device:TPU:0, one launch (start us, length us, event | category | flops | bytes accessed | tf_op | source)
XLA Modules:
  0.0 63.9 jit_solution(6800139697767756301)
XLA Ops:
  0.0 62.0 %shard_map.100 = bf16[128,2048]{1,0:T(8,128)(2,1)} custom-call(s32[2,128]{1,0:T(2,128)} %bitcast.12, f32[2,128]{1,0:T(2,128)} %bitcast.13, bf16[128,2048]{1,0:T(8,128)(2,1)} %tokens_ref.1, f32[1,2048]{1,0:T(1,128)} %bitcast.10, f32[1,2048]{1,0:T(1,128)} %bitcast.11, bf16[128,256]{1,0:T(8,128)(2,1)} %din_ref.1, bf16[128,256]{1,0:T(8,128)(2,1)} %dout_ref.1, ...), custom_call_target="tpu_custom_call" | custom-call | tf_op jit(solution)/shard_map/pallas_call | solution.py:1133
  62.0 1.9 %copy.12 = bf16[128,2048]{1,0:T(8,128)(2,1)} copy(bf16[128,2048]{1,0:T(8,128)(2,1)} %shard_map.100) | data formatting | bytes 1048576
